TPU v7x, 512 devices: a whole 4x4x16 slice. The times are simulated.
512 devices in a mesh: fs: 64 (over z, y), tp: 8 (over x, core).
Axes of the slice: x: 4, y: 4, z: 16, core: 2. Of those that a mesh axis runs over, the one named last changes fastest.
Arguments:
- tokens: bfloat16 [32768, 2048], P('fs'), may hold values from -6 to 6
- norm_gain: float32 [2048], P('fs'), may hold values from 0.1 to 1.9
- w_gate: float32 [64, 2048, 512], P(None, 'fs', 'tp'), may hold values from -0.125 to 0.125
- w_up: float32 [64, 2048, 512], P(None, 'fs', 'tp'), may hold values from -0.125 to 0.125
- w_down: float32 [64, 2048, 512], P(None, 'fs', 'tp'), may hold values from -0.25 to 0.25
- route_expert: int32 [32768, 2], P('fs'), may hold values from 0 to 63, as said below
- group_prob: float32 [32768], P('fs'), may hold values from 0.25 to 1
- pair_logit: float32 [32768, 2], P('fs'), may hold values from -6 to 6
Outputs:
- new_gate: bfloat16 [64, 2048, 512], P('fs', None, 'tp')
- new_up: bfloat16 [64, 2048, 512], P('fs', None, 'tp')
- new_down: bfloat16 [64, 2048, 512], P('fs', None, 'tp')
- mixed: bfloat16 [32768, 2048], P('fs', 'tp')
Inputs may be any that keep to these rules, and one draw needn't show every extreme that they name: `route_expert`: each row names two different experts of one group: for its group g both lie in g * 8 to g * 8 + 7, one of 8 groups. In each aligned block of 512 rows every expert is named by exactly 16 rows, half of them in each column.
All inputs are finite; a program needn't handle non-finite values.
Results may differ from a plain program's by a relative error of at most 0.014.
Values may be sent and summed in bfloat16 or wider, within the bound.
No kernel may reach another device: no remote copies, remote signals or barrier semaphores. Data moves between devices by JAX's collectives and lax.ppermute only.
A program may use at most 64 MiB of HBM per device.

v0:
```python
import jax
import jax.numpy as jnp
from jax import lax
from jax.sharding import PartitionSpec as P

D = 2048
TOP = 2


EPSILON = 1e-06


def in_one_piece(arrays, axis, split_dim, concat_dim, along):
    both = jnp.concatenate(arrays, axis=along)
    filled, at, outs = (
        lax.all_to_all(both, axis, split_axis=split_dim, concat_axis=concat_dim, tiled=True),
        0,
        [],
    )
    for a in arrays:
        outs.append(lax.slice_in_dim(filled, at, at + a.shape[along], axis=along))
        at += a.shape[along]
    return tuple(outs)


def local(tokens, norm_gain, w_gate, w_up, w_down, route_expert, group_prob, pair_logit):
    expert_count = lax.axis_size("fs")
    column_count = lax.axis_size("tp")
    row_scale = norm_gain[None, :, None]
    gate_local = (w_gate * row_scale).astype(jnp.bfloat16)
    up_local = (w_up * row_scale).astype(jnp.bfloat16)
    down_local = w_down.astype(jnp.bfloat16)
    new_gate, new_up, new_down = in_one_piece((gate_local, up_local, down_local), "fs", 0, 1, 2)
    widened = tokens.astype(jnp.float32)
    normed = (
        widened * lax.rsqrt(jnp.mean(widened * widened, axis=1, keepdims=True) + EPSILON)
    ).astype(jnp.bfloat16)
    flat_ids = route_expert.reshape(-1)
    assigned = flat_ids.shape[0]
    capacity = assigned // expert_count
    one_hot = (flat_ids[:, None] == jnp.arange(expert_count, dtype=jnp.int32)[None, :]).astype(
        jnp.int32
    )
    slot_rank = jnp.sum((jnp.cumsum(one_hot, axis=0) - one_hot) * one_hot, axis=1)
    dest_slot = flat_ids * capacity + slot_rank
    row_source = (
        jnp.zeros((assigned,), jnp.int32)
        .at[dest_slot]
        .set(jnp.arange(assigned, dtype=jnp.int32) // TOP)
    )
    outgoing = normed[row_source].reshape(expert_count, capacity, D)
    gate_matrix = new_gate[0]
    up_matrix = new_up[0]
    slice_width = D // column_count
    own_slice = lax.dynamic_slice_in_dim(
        outgoing, lax.axis_index("tp") * slice_width, slice_width, 2
    )
    received = lax.all_to_all(own_slice, "fs", split_axis=0, concat_axis=0, tiled=True).reshape(
        assigned, slice_width
    )
    segment = lax.all_gather(received, "tp", axis=1, tiled=True)
    gate_pre = jnp.dot(segment, gate_matrix, preferred_element_type=jnp.float32)
    up_pre = jnp.dot(segment, up_matrix, preferred_element_type=jnp.float32)
    hidden = (jax.nn.silu(gate_pre) * up_pre).astype(jnp.bfloat16)
    partial_out = lax.dot_general(
        hidden, new_down[0], (((1,), (1,)), ((), ())), preferred_element_type=jnp.float32
    )
    summed = lax.psum_scatter(
        partial_out.reshape(expert_count, capacity, D).astype(jnp.bfloat16),
        "tp",
        scatter_dimension=2,
        tiled=True,
    )
    returned = lax.all_to_all(summed, "fs", split_axis=0, concat_axis=0, tiled=True)
    per_slot = (
        returned.reshape(assigned, -1)[dest_slot]
        .reshape(tokens.shape[0], TOP, -1)
        .astype(jnp.float32)
    )
    logit_gap = pair_logit[:, 0] - pair_logit[:, 1]
    weight_first = group_prob * jax.nn.sigmoid(logit_gap)
    weight_second = group_prob * jax.nn.sigmoid(-logit_gap)
    mixed = (
        weight_first[:, None] * per_slot[:, 0] + weight_second[:, None] * per_slot[:, 1]
    ).astype(jnp.bfloat16)
    return (new_gate, new_up, new_down, mixed)


def solution(mesh):
    placed = (
        P("fs", None),
        P("fs"),
        P(None, "fs", "tp"),
        P(None, "fs", "tp"),
        P(None, "fs", "tp"),
        P("fs", None),
        P("fs"),
        P("fs", None),
    )
    return jax.shard_map(
        local,
        mesh=mesh,
        in_specs=placed,
        out_specs=(P("fs", None, "tp"), P("fs", None, "tp"), P("fs", None, "tp"), P("fs", "tp")),
        check_vma=False,
    )
```

profile of v0, /device:TPU:7, one launch (start us, length us, event | category | flops | bytes accessed | tf_op | source)
XLA Modules:
  0.0 260.3 jit_solution(13213390310283078784)
XLA Ops:
  7.2 0.0 copy-start.1
  7.2 0.0 all-gather.2.cloned.1.call-start
  7.2 1.0 copy.18
  8.2 0.2 eq.29
  8.4 0.2 eq.25
  8.5 0.7 broadcast_multiply_fusion
  9.3 18.0 %reduce-window.6 = s32[64,8,128]{2,1,0:T(8,128)S(1)} reduce-window(s32[64,8,128]{2,1,0:T(8,128)S(1)} %fusion.14, s32[]{:T(128)} %constant.38.clone.1), window={size=1x1x128 pad=0_0x0_0x127_0}, to_apply=%region_1.0 | reduce-window | flops 8323072 | bytes 524292 | tf_op jit(solution)/shard_map/reduce-window
  27.3 0.1 slice.43
  27.4 0.1 copy.20
  27.6 0.1 copy.21
  27.7 0.1 broadcast_add_fusion
  27.8 0.1 copy.17
  28.0 0.2 mul.86
  28.2 0.1 fusion.13
  28.2 4.3 %scatter_custom_fusion = s32[1024]{0:T(1024)S(1)} fusion(s32[1024]{0:T(1024)S(1)} %bitcast.66, s32[1024]{0:T(1024)S(1)} %add_select_fusion, s32[]{:T(128)} %constant.38.clone.1), kind=kCustom, calls=%fused_computation.44 | custom fusion | bytes 4100 | tf_op jit(solution)/shard_map/scatter | solution.py:49
  32.6 0.0 copy-done.1
  32.6 0.5 fusion
  33.1 2.0 fusion.1
  35.1 0.0 copy-start.2
  35.1 6.0 %gather_fusion = bf16[1024,2048]{1,0:T(8,128)(2,1)} fusion(bf16[512,2048]{1,0:T(8,128)(2,1)S(1)} %fusion.1, s32[1024]{0:T(1024)S(1)} %fusion.17), kind=kCustom, calls=%fused_computation | custom fusion | bytes 8392704 | tf_op jit(solution)/shard_map/gather | solution.py:51
  41.1 0.0 copy-start.3
  41.1 0.0 copy-start.4
  41.1 0.0 copy-start.7
  41.1 1.2 constant_dynamic-slice_fusion
  42.3 49.3 %all_to_all.22 = bf16[64,16,256]{2,1,0:T(8,128)(2,1)} all-to-all(bf16[64,16,256]{2,1,0:T(8,128)(2,1)S(1)} %constant_dynamic-slice_fusion), channel_id=1, replica_groups=mesh['fs'=64,'tp'=8] {'fs'}, dimensions={0} | all-to-all | bytes 1048576 | tf_op jit(solution)/shard_map/all_to_all | solution.py:58
  91.6 0.0 all-gather.2.cloned.1.call-update
  91.7 0.0 reduce-scatter.2.cloned.1.call-start
  91.7 0.0 copy-done.2
  91.7 0.1 convert_element_type.39
  91.8 0.0 copy-done.3
  91.8 0.0 copy-done.4
  91.8 0.0 copy-done.7
  91.8 0.3 multiply_convert_fusion.1
  92.1 0.6 pad_maximum_fusion
  92.7 57.9 %all_to_all.23 = bf16[64,32,192]{2,1,0:T(8,128)(2,1)S(1)} all-to-all(bf16[64,32,192]{2,1,0:T(8,128)(2,1)S(1)} %pad_maximum_fusion), channel_id=1, replica_groups=mesh['fs'=64,'tp'=8] {'fs'}, dimensions={0} | all-to-all | bytes 1572864 | tf_op jit(solution)/shard_map/all_to_all | solution.py:16
  150.6 0.0 all-gather.2.cloned.1.call-done
  150.7 0.0 copy-start
  150.7 3.7 %fusion.9 = f32[1024,64]{0,1:T(8,128)S(1)} fusion(bf16[1024,2048]{1,0:T(8,128)(2,1)} %all-gather.2.cloned.1.call-done, bf16[1,2048,192]{2,1,0:T(8,128)(2,1)S(1)} %bitcast.56), kind=kOutput, calls=%fused_computation.21 | convolution fusion | flops 268435456 | bytes 4980736 | tf_op jit(solution)/shard_map/dot_general | solution.py:62
  154.4 0.0 copy-done
  154.4 1.5 fusion.2
  155.9 0.2 copy.22
  156.0 0.0 copy-start.5
  156.1 0.0 copy-start.6
  156.1 3.2 %convolution_convert_fusion = bf16[64,16,2048]{2,1,0:T(8,128)(2,1)} fusion(bf16[64,16,64]{2,1,0:T(8,128)(2,1)S(1)} %bitcast.62, bf16[1,2048,192]{2,1,0:T(8,128)(2,1)S(1)} %bitcast.58), kind=kOutput, calls=%fused_computation.7 | convolution fusion | flops 270532608 | bytes 4980736 | tf_op jit(solution)/shard_map/dot_general | solution.py:65
  159.3 0.0 reduce-scatter.2.cloned.1.call-update
  159.3 41.0 %reduce-scatter.2.cloned.1.call-done = bf16[64,16,256]{2,1,0:T(8,128)(2,1)} async-done(((bf16[64,16,2048]{2,1,0:T(8,128)(2,1)}), bf16[64,16,256]{2,1,0:T(8,128)(2,1)}) %reduce-scatter.2.cloned.1.call-update) | async-done | bytes 524304 | tf_op jit(solution)/shard_map/reduce_scatter | solution.py:68
  200.3 14.6 %all-to-all-start.2 = ((bf16[64,16,256]{2,1,0:T(8,128)(2,1)}), bf16[64,16,256]{2,1,0:T(8,128)(2,1)S(1)}, u32[]{:S(2)}, u32[]{:S(2)}) async-start(bf16[64,16,256]{2,1,0:T(8,128)(2,1)} %reduce-scatter.2.cloned.1.call-done), calls=%async_computation.3 | async-start | bytes 1048576 | tf_op jit(solution)/shard_map/all_to_all | solution.py:74
  214.9 0.0 copy-done.5
  215.0 0.0 copy-done.6
  215.0 0.3 fusion.25
  215.4 0.9 copy.25
  216.3 0.9 copy.26
  217.2 0.9 copy.27
  218.1 29.2 %all-to-all-done.2 = bf16[64,16,256]{2,1,0:T(8,128)(2,1)S(1)} async-done(((bf16[64,16,256]{2,1,0:T(8,128)(2,1)}), bf16[64,16,256]{2,1,0:T(8,128)(2,1)S(1)}, u32[]{:S(2)}, u32[]{:S(2)}) %all-to-all-start.2) | async-done | bytes 524320 | tf_op jit(solution)/shard_map/all_to_all | solution.py:74
  247.3 3.9 %gather_fusion.1 = bf16[1024,256]{1,0:T(8,128)(2,1)S(1)} fusion(bf16[1024,256]{1,0:T(8,128)(2,1)S(1)} %bitcast.55, s32[1024]{0:T(1024)S(1)} %broadcast_clamp_fusion), kind=kCustom, calls=%fused_computation.1 | custom fusion | bytes 1052672 | tf_op jit(solution)/shard_map/gather | solution.py:76
  251.2 0.5 reshape.98
  251.8 0.8 fusion.24
  252.6 0.9 fusion.6
  (11 shorter events, 0.1 us)
Async XLA Ops:
  7.2 25.4 %copy-start.1 = (bf16[512,2048]{1,0:T(8,128)(2,1)S(1)}, bf16[512,2048]{1,0:T(8,128)(2,1)}, u32[]{:S(2)}) copy-start(bf16[512,2048]{1,0:T(8,128)(2,1)} %param.8) | copy-start | bytes 6291460
  7.2 143.5 %all-gather.2.cloned.1.call-start = ((), (), s32[]{:S(2)}) async-start(), calls=%async_computation.4 | async-start | bytes 4718592 | tf_op jit(solution)/shard_map/all_gather | solution.py:61
  35.1 56.6 %copy-start.2 = (f32[64,32,64]{2,1,0:T(8,128)S(1)}, f32[64,32,64]{2,1,0:T(8,128)}, u32[]{:S(2)}) copy-start(f32[64,32,64]{2,1,0:T(8,128)} %param.12) | copy-start | bytes 1572868
  41.1 50.7 %copy-start.3 = (f32[64,32,64]{2,1,0:T(8,128)S(1)}, f32[64,32,64]{2,1,0:T(8,128)}, u32[]{:S(2)}) copy-start(f32[64,32,64]{2,1,0:T(8,128)} %param.10) | copy-start | bytes 1572868
  41.1 50.7 %copy-start.4 = (f32[64,32,64]{2,1,0:T(8,128)S(1)}, f32[64,32,64]{2,1,0:T(8,128)}, u32[]{:S(2)}) copy-start(f32[64,32,64]{2,1,0:T(8,128)} %param.11) | copy-start | bytes 1572868
  41.1 50.7 %copy-start.7 = (f32[32]{0:T(128)S(1)}, f32[32]{0:T(128)}, u32[]{:S(2)}) copy-start(f32[32]{0:T(128)} %param.9) | copy-start | bytes 388
  91.7 108.6 %reduce-scatter.2.cloned.1.call-start = ((), (), s32[]{:S(2)}) async-start(), calls=%async_computation.5 | async-start | bytes 4718592 | tf_op jit(solution)/shard_map/reduce_scatter | solution.py:68
  150.7 3.7 %copy-start = (bf16[1024,2048]{1,0:T(8,128)(2,1)S(1)}, bf16[1024,2048]{1,0:T(8,128)(2,1)}, u32[]{:S(2)}) copy-start(bf16[1024,2048]{1,0:T(8,128)(2,1)} %all-gather.2.cloned.1.call-done) | copy-start | bytes 12582916
  156.0 58.9 %copy-start.5 = (f32[512,2]{0,1:T(2,128)S(1)}, f32[512,2]{0,1:T(2,128)}, u32[]{:S(2)}) copy-start(f32[512,2]{0,1:T(2,128)} %param.15) | copy-start | bytes 12292
  156.1 58.9 %copy-start.6 = (f32[512]{0:T(512)S(1)}, f32[512]{0:T(512)}, u32[]{:S(2)}) copy-start(f32[512]{0:T(512)} %param.14) | copy-start | bytes 6148
  200.3 47.0 %all-to-all-start.2 = ((bf16[64,16,256]{2,1,0:T(8,128)(2,1)}), bf16[64,16,256]{2,1,0:T(8,128)(2,1)S(1)}, u32[]{:S(2)}, u32[]{:S(2)}) async-start(bf16[64,16,256]{2,1,0:T(8,128)(2,1)} %reduce-scatter.2.cloned.1.call-done), calls=%async_computation.3 | async-start | bytes 1048576 | tf_op jit(solution)/shard_map/all_to_all | solution.py:74
Sparse Core Ops, SparseCore 0:
  91.8 36.6 all-gather.1
  159.4 40.8 reduce-scatter.1
where the time goes:
time: 261 us; the launch traced here: 260 us
  blocking collectives  107 us (41%)
  waiting for transfers between devices  70.3 us (27%)
  other arithmetic  23.4 us (9%)
  local copies, waits for them, and re-layouts  22 us (8%)
  starting transfers between devices  14.7 us (6%)
  between operations  14.3 us (5%)
  matrix products  8.4 us (3%)
    all_to_all x1, blocking collectives, in_one_piece(): lax.all_to_all(both, axis, split_axis=split_dim, concat_axis=concat_dim,...  57.9 us
    all_to_all x1, blocking collectives, local(): lax.all_to_all(own_slice, 'fs', split_axis=0, concat_axis=0, tiled=True)  49.3 us
    reduce_scatter x1, waiting for transfers between devices, local(): lax.psum_scatter(partial_out.reshape(expert_count, capacity, D).astype(jn...  41 us
    all_to_all x1, waiting for transfers between devices, local(): lax.all_to_all(summed, 'fs', split_axis=0, concat_axis=0, tiled=True)  29.2 us
    another operation x3, other arithmetic  18.2 us
    all_to_all x1, starting transfers between devices, local(): lax.all_to_all(summed, 'fs', split_axis=0, concat_axis=0, tiled=True)  14.6 us
    gather x1, local copies, waits for them, and re-layouts, local(): outgoing = normed[row_source].reshape(expert_count, capacity, D)  5.99 us
  transfers between devices with their start and end apart: 3, of which 2 were waited for; matrix products, arithmetic and copies ran while one was open for 2% of the time, Pallas kernels for 0%

commit v1 on v0

v1 whole, which is shorter than its diff:
```python
import jax
import jax.numpy as jnp
from jax import lax
from jax.experimental import pallas as pl
from jax.experimental.pallas import tpu as pltpu
from jax.sharding import Mesh, PartitionSpec as P

D = 2048
EPSILON = 1e-06
FS = ("g", "l", "y")
TP = ("x", "c")
IN_GROUP = ("l", "y", "x", "c")
BF = jnp.bfloat16
F32 = jnp.float32


def expert_kernel(*refs):
    x_ref, shards, out_ref, acc = refs[0], refs[1:-2], refs[-2], refs[-1]
    x = x_ref[...]
    groups = [(r,) for r in shards[:6]] + [shards[6:8], shards[8:10]]

    def gate_up(group):
        return jnp.concatenate([r[:, :32, :].reshape(-1, 128) for r in group], axis=0)

    def down(group):
        return jnp.concatenate([r[:, 32:, :].reshape(-1, 128) for r in group], axis=0)

    lane = lax.broadcasted_iota(jnp.int32, (128, 256), 1) % 128
    low = lane < 64
    for k in range(4):
        a, b = groups[2 * k], groups[2 * k + 1]
        both = jnp.concatenate([gate_up(a), gate_up(b)], axis=1)
        pre = jnp.dot(x, both, preferred_element_type=F32)
        other = jnp.concatenate(
            [pltpu.roll(pre[:, :128], 64, 1), pltpu.roll(pre[:, 128:], 64, 1)], axis=1
        )
        gate = jnp.where(low, pre, other)
        up = jnp.where(low, other, pre)
        hidden = gate / (1.0 + jnp.exp(-gate)) * up
        stacked = jnp.concatenate(
            [jnp.where(low, hidden, 0.0), jnp.where(low, 0.0, hidden)], axis=0
        ).astype(BF)
        down_pair = jnp.concatenate([down(a), down(b)], axis=1)
        part = lax.dot_general(
            stacked, down_pair, (((1,), (1,)), ((), ())), preferred_element_type=F32
        )
        if k == 0:
            acc[...] = part
        else:
            acc[...] += part
    for j in range(8):
        for t in range(8):
            for h in range(2):
                out_ref[8 * j + t, :, 128 * h : 128 * (h + 1)] = acc[
                    128 * h + 16 * j : 128 * h + 16 * (j + 1), 128 * t : 128 * (t + 1)
                ].astype(BF)


def expert(rows, shards):
    return pl.pallas_call(
        expert_kernel,
        out_shape=jax.ShapeDtypeStruct((64, 16, 256), BF),
        scratch_shapes=[pltpu.VMEM((256, 1024), F32)],
        name="expert",
    )(rows, *shards)


def gather_weights(own):
    def along_x(v, by):
        return lax.ppermute(v, "x", [(i, (i + by) % 4) for i in range(4)])

    def swap(v):
        return lax.ppermute(v, "c", [(0, 1), (1, 0)])

    left = along_x(own, 1)
    right = along_x(own, -1)
    own_c = swap(own)
    far_a = along_x(left[:32], 1)
    far_b = along_x(right[32:], -1)
    left_c, right_c = swap(left), swap(right)
    far_a_c, far_b_c = swap(far_a), swap(far_b)
    return (own, left, right, own_c, left_c, right_c, far_a, far_b, far_a_c, far_b_c)


def local(tokens, norm_gain, w_gate, w_up, w_down, route_expert, group_prob, pair_logit):
    scale = norm_gain[None, :, None]
    gate_up = jnp.concatenate([w_gate * scale, w_up * scale], axis=2).astype(BF)
    down = jnp.concatenate([w_down[:, :16], w_down[:, 16:]], axis=2).astype(BF)
    packed = jnp.concatenate([gate_up, down], axis=1)
    own = lax.all_to_all(packed, FS, split_axis=0, concat_axis=0, tiled=True)
    new_gate = own[:, :32, :64].reshape(1, D, 64)
    new_up = own[:, :32, 64:].reshape(1, D, 64)
    new_down = jnp.concatenate([own[:, 32:, :64], own[:, 32:, 64:]], axis=1).reshape(1, D, 64)

    my_share = lax.axis_index(TP)
    first, second = route_expert[:, 0], route_expert[:, 1]
    group = first // 8
    experts = jnp.arange(64, dtype=jnp.int32)
    hot_first = first[:, None] == experts[None, :]
    hot_second = second[:, None] == experts[None, :]
    named = (hot_first | hot_second).astype(BF)
    row_at = jnp.arange(512, dtype=jnp.int32)
    before = (row_at[None, :] < row_at[:, None]).astype(BF)
    earlier = jnp.dot(before, named, preferred_element_type=F32)
    rank_first = jnp.sum(jnp.where(hot_first, earlier, 0.0), axis=1).astype(jnp.int32)
    rank_second = jnp.sum(jnp.where(hot_second, earlier, 0.0), axis=1).astype(jnp.int32)
    same_group = group[:, None] == experts[None, :] // 8
    rank_group = (jnp.sum(jnp.where(same_group, earlier, 0.0), axis=1) * 0.5).astype(jnp.int32)
    slot = group * 64 + rank_group

    def send_at(e, rank):
        return jnp.where(rank // 2 == my_share, ((e % 8) * 8 + e // 8) * 2 + rank % 2, -1)

    send_rows = jnp.arange(128, dtype=jnp.int32)[:, None]
    pick = (
        (send_at(first, rank_first)[None, :] == send_rows)
        | (send_at(second, rank_second)[None, :] == send_rows)
    ).astype(BF)
    chosen = jnp.dot(pick, tokens, preferred_element_type=F32)
    normed = (
        chosen * lax.rsqrt(jnp.mean(chosen * chosen, axis=1, keepdims=True) + EPSILON)
    ).astype(BF)
    received = lax.all_to_all(
        normed.reshape(64, 32, 128), ("l", "y", "g"), split_axis=0, concat_axis=0, tiled=True
    )

    gap = pair_logit[:, 0] - pair_logit[:, 1]
    weight_first = group_prob * jax.nn.sigmoid(gap)
    weight_second = group_prob * jax.nn.sigmoid(-gap)
    high_first = lax.reduce_precision(weight_first, 8, 7)
    high_second = lax.reduce_precision(weight_second, 8, 7)
    facts = jnp.stack(
        [
            ((first % 8) * 16 + rank_first).astype(F32),
            ((second % 8) * 16 + rank_second).astype(F32),
            high_first,
            high_second,
            weight_first - high_first,
            weight_second - high_second,
            jnp.zeros_like(gap),
            jnp.zeros_like(gap),
        ]
    ).astype(BF)
    to_slot = (slot[:, None] == row_at[None, :]).astype(BF)
    facts = jnp.dot(facts, to_slot, preferred_element_type=F32).astype(BF)
    facts = facts.reshape(8, 8, 64).transpose(1, 0, 2)
    facts = lax.all_to_all(facts, "g", split_axis=0, concat_axis=0, tiled=True)
    facts = facts.transpose(1, 0, 2).reshape(8, 512).astype(F32)
    code = facts[:2].astype(jnp.int32)
    source = row_at // 64
    at = (code // 16 * 8 + code % 16 // 2) * 16 + source[None, :] * 2 + code % 2
    slots = jnp.arange(1024, dtype=jnp.int32)[:, None]
    is_first, is_second = at[0][None, :] == slots, at[1][None, :] == slots
    mix_high = jnp.where(is_first, facts[2][None, :], jnp.where(is_second, facts[3][None, :], 0.0))
    mix_low = jnp.where(is_first, facts[4][None, :], jnp.where(is_second, facts[5][None, :], 0.0))
    mix_high, mix_low = mix_high.astype(BF), mix_low.astype(BF)

    shards = gather_weights(own)
    outs = expert(received.reshape(128, D), shards)
    back = lax.all_to_all(outs, IN_GROUP, split_axis=0, concat_axis=0, tiled=True)
    back = back.reshape(1024, 256)
    over_slots = (((0,), (0,)), ((), ()))
    mixed = (
        lax.dot_general(mix_high, back, over_slots, preferred_element_type=F32)
        + lax.dot_general(mix_low, back, over_slots, preferred_element_type=F32)
    ).astype(BF)
    home = lax.all_to_all(
        mixed.reshape(8, 64, 256), "g", split_axis=0, concat_axis=0, tiled=True
    ).reshape(512, 256)
    home = jnp.dot(to_slot, home, preferred_element_type=F32).astype(BF)
    feature = jnp.arange(256, dtype=jnp.int32)
    lies_at = (feature // 16 % 2) * 128 + feature // 32 * 16 + feature % 16
    reorder = (lies_at[None, :] == feature[:, None]).astype(BF)
    home = jnp.dot(home, reorder, preferred_element_type=F32).astype(BF)
    return new_gate, new_up, new_down, home


def solution(mesh):
    fine = Mesh(mesh.devices.reshape(8, 2, 4, 4, 2), ("g", "l", "y", "x", "c"))
    placed = (
        P(FS, None),
        P(FS),
        P(None, FS, TP),
        P(None, FS, TP),
        P(None, FS, TP),
        P(FS, None),
        P(FS),
        P(FS, None),
    )
    return jax.shard_map(
        local,
        mesh=fine,
        in_specs=placed,
        out_specs=(P(FS, None, TP), P(FS, None, TP), P(FS, None, TP), P(FS, TP)),
        check_vma=False,
    )
```

time: 261 us -> 191 us (0.73)
  the two profiles are of different devices: /device:TPU:7 before, /device:TPU:1 now
where the time goes in v1:
time: 191 us; the launch traced here: 190 us
  starting transfers between devices  82.1 us (43%)
  waiting for transfers between devices  80.7 us (42%)
  local copies, waits for them, and re-layouts  12.4 us (6%)
  Pallas kernels  5.4 us (3%)
  matrix products  5.22 us (3%)
  other arithmetic  3.51 us (2%)
    all_to_all x1, waiting for transfers between devices, local(): own = lax.all_to_all(packed, FS, split_axis=0, concat_axis=0, tiled=True)  38.7 us
    all_to_all x1, starting transfers between devices, local(): own = lax.all_to_all(packed, FS, split_axis=0, concat_axis=0, tiled=True)  19.3 us
    ppermute x5, starting transfers between devices, swap(): return lax.ppermute(v, 'c', [(0, 1), (1, 0)])  15.3 us
    all_to_all x1, waiting for transfers between devices, local(): lax.all_to_all(mixed.reshape(8, 64, 256), 'g', split_axis=0, concat_axis=...  15.2 us
    ppermute x4, starting transfers between devices, along_x(): return lax.ppermute(v, 'x', [(i, (i + by) % 4) for i in range(4)])  13 us
    all_to_all x1, waiting for transfers between devices, local(): lax.all_to_all(outs, IN_GROUP, split_axis=0, concat_axis=0, tiled=True)  11.6 us
    all_to_all x1, starting transfers between devices, local(): facts = lax.all_to_all(facts, 'g', split_axis=0, concat_axis=0, tiled=True)  10.7 us
    ppermute x4, waiting for transfers between devices, along_x(): return lax.ppermute(v, 'x', [(i, (i + by) % 4) for i in range(4)])  10.3 us
  transfers between devices with their start and end apart: 14, of which 5 were waited for; matrix products, arithmetic and copies ran while one was open for 7% of the time, Pallas kernels for 3%

profile of v1, /device:TPU:1, one launch (start us, length us, event | category | flops | bytes accessed | tf_op | source)
XLA Modules:
  0.0 190.4 jit_solution(9160301568985804129)
XLA Ops:
  0.6 0.0 copy-start
  0.6 0.0 copy-start.3
  0.7 0.0 copy-start.4
  0.7 1.5 convert.39
  2.2 0.1 copy-done.3
  2.3 0.3 copy-done.4
  2.7 0.3 multiply_convert_fusion.2
  3.0 0.0 copy-start.5
  3.0 1.3 maximum_maximum_fusion
  4.3 19.3 %all-to-all-start = ((bf16[64,48,128]{2,1,0:T(8,128)(2,1)}), bf16[64,48,128]{2,1,0:T(8,128)(2,1)S(1)}, u32[]{:S(2)}, u32[]{:S(2)}) async-start(bf16[64,48,128]{2,1,0:T(8,128)(2,1)} %maximum_maximum_fusion), calls=%async_computation | async-start | bytes 1572864 | tf_op jit(solution)/shard_map/all_to_all | solution.py:90
  23.6 0.3 select_reduce_fusion.2
  24.0 0.5 multiply_reduce_fusion
  24.5 0.1 multiply_convert_fusion
  24.6 0.0 copy-start.7
  24.7 1.0 reshape.452
  25.7 38.7 %all-to-all-done.refs_1_ = bf16[64,48,128]{2,1,0:T(8,128)(2,1)S(1)} async-done(((bf16[64,48,128]{2,1,0:T(8,128)(2,1)}), bf16[64,48,128]{2,1,0:T(8,128)(2,1)S(1)}, u32[]{:S(2)}, u32[]{:S(2)}) %all-to-all-start) | async-done | bytes 786464 | tf_op jit(solution)/shard_map/all_to_all | solution.py:90
  64.4 8.6 %all-to-all-start.2 = ((bf16[64,32,128]{2,1,0:T(8,128)(2,1)}), bf16[64,32,128]{2,1,0:T(8,128)(2,1)S(1)}, u32[]{:S(2)}, u32[]{:S(2)}) async-start(bf16[64,32,128]{2,1,0:T(8,128)(2,1)} %reshape.452), calls=%async_computation.2 | async-start | bytes 1048576 | tf_op jit(solution)/shard_map/all_to_all | solution.py:123
  73.0 3.1 %collective-permute-start = (bf16[64,48,128]{2,1,0:T(8,128)(2,1)S(1)}, bf16[64,48,128]{2,1,0:T(8,128)(2,1)}, u32[]{:S(2)}, u32[]{:S(2)}) collective-permute-start(bf16[64,48,128]{2,1,0:T(8,128)(2,1)S(1)} %all-to-all-done.refs_1_), channel_id=1, source_target_pairs={{0,2},{2,4},{4,6},{6,0},{1,3},{3,5},{5,7},{7,1},{8,10},{10,12},{12... | collective-permute-start | bytes 2359304 | tf_op jit(solution)/shard_map/ppermute | solution.py:70
  76.1 3.4 %collective-permute-start.1 = (bf16[64,48,128]{2,1,0:T(8,128)(2,1)S(1)}, bf16[64,48,128]{2,1,0:T(8,128)(2,1)}, u32[]{:S(2)}, u32[]{:S(2)}) collective-permute-start(bf16[64,48,128]{2,1,0:T(8,128)(2,1)S(1)} %all-to-all-done.refs_1_), channel_id=1, source_target_pairs={{0,6},{2,0},{4,2},{6,4},{1,7},{3,1},{5,3},{7,5},{8,14},{10,8},{12,... | collective-permute-start | bytes 2359304 | tf_op jit(solution)/shard_map/ppermute | solution.py:70
  79.6 3.9 %collective-permute-start.2 = (bf16[64,48,128]{2,1,0:T(8,128)(2,1)S(1)}, bf16[64,48,128]{2,1,0:T(8,128)(2,1)}, u32[]{:S(2)}, u32[]{:S(2)}) collective-permute-start(bf16[64,48,128]{2,1,0:T(8,128)(2,1)S(1)} %all-to-all-done.refs_1_), channel_id=1, source_target_pairs={{0,1},{1,0},{2,3},{3,2},{4,5},{5,4},{6,7},{7,6},{8,9},{9,8},{10,11... | collective-permute-start | bytes 2359304 | tf_op jit(solution)/shard_map/ppermute | solution.py:73
  83.5 10.3 %collective-permute-done.refs_2_ = bf16[64,48,128]{2,1,0:T(8,128)(2,1)} collective-permute-done((bf16[64,48,128]{2,1,0:T(8,128)(2,1)S(1)}, bf16[64,48,128]{2,1,0:T(8,128)(2,1)}, u32[]{:S(2)}, u32[]{:S(2)}) %collective-permute-start) | collective-permute-done | bytes 786464 | tf_op jit(solution)/shard_map/ppermute | solution.py:70
  93.8 1.8 slice.94
  95.6 1.9 %collective-permute-start.5 = (bf16[32,48,128]{2,1,0:T(8,128)(2,1)}, bf16[32,48,128]{2,1,0:T(8,128)(2,1)}, u32[]{:S(2)}, u32[]{:S(2)}) collective-permute-start(bf16[32,48,128]{2,1,0:T(8,128)(2,1)} %slice.94), channel_id=1, source_target_pairs={{0,2},{2,4},{4,6},{6,0},{1,3},{3,5},{5,7},{7,1},{8,10},{10,12},{12... | collective-permute-start | bytes 1179656 | tf_op jit(solution)/shard_map/ppermute | solution.py:70
  97.5 0.0 collective-permute-done.1.refs_3_
  97.5 1.8 slice.95
  99.3 4.6 %collective-permute-start.6 = (bf16[32,48,128]{2,1,0:T(8,128)(2,1)}, bf16[32,48,128]{2,1,0:T(8,128)(2,1)}, u32[]{:S(2)}, u32[]{:S(2)}) collective-permute-start(bf16[32,48,128]{2,1,0:T(8,128)(2,1)} %slice.95), channel_id=1, source_target_pairs={{0,6},{2,0},{4,2},{6,4},{1,7},{3,1},{5,3},{7,5},{8,14},{10,8},{12,... | collective-permute-start | bytes 1179656 | tf_op jit(solution)/shard_map/ppermute | solution.py:70
  103.9 4.8 %collective-permute-start.3 = (bf16[64,48,128]{2,1,0:T(8,128)(2,1)}, bf16[64,48,128]{2,1,0:T(8,128)(2,1)}, u32[]{:S(2)}, u32[]{:S(2)}) collective-permute-start(bf16[64,48,128]{2,1,0:T(8,128)(2,1)} %collective-permute-done.refs_2_), channel_id=1, source_target_pairs={{0,1},{1,0},{2,3},{3,2},{4,5},{5,4},{6,7},{7,6},{8,9},{9,8},{10,11... | collective-permute-start | bytes 2359304 | tf_op jit(solution)/shard_map/ppermute | solution.py:73
  108.6 1.9 %collective-permute-start.4 = (bf16[64,48,128]{2,1,0:T(8,128)(2,1)}, bf16[64,48,128]{2,1,0:T(8,128)(2,1)}, u32[]{:S(2)}, u32[]{:S(2)}) collective-permute-start(bf16[64,48,128]{2,1,0:T(8,128)(2,1)} %collective-permute-done.1.refs_3_), channel_id=1, source_target_pairs={{0,1},{1,0},{2,3},{3,2},{4,5},{5,4},{6,7},{7,6},{8,9},{9,8},{10,11... | collective-permute-start | bytes 2359304 | tf_op jit(solution)/shard_map/ppermute | solution.py:73
  110.7 0.0 collective-permute-done.5.refs_7_
  110.7 2.4 %collective-permute-start.7 = (bf16[32,48,128]{2,1,0:T(8,128)(2,1)}, bf16[32,48,128]{2,1,0:T(8,128)(2,1)}, u32[]{:S(2)}, u32[]{:S(2)}) collective-permute-start(bf16[32,48,128]{2,1,0:T(8,128)(2,1)} %collective-permute-done.5.refs_7_), channel_id=1, source_target_pairs={{0,1},{1,0},{2,3},{3,2},{4,5},{5,4},{6,7},{7,6},{8,9},{9,8},{10,11... | collective-permute-start | bytes 1179656 | tf_op jit(solution)/shard_map/ppermute | solution.py:73
  113.1 0.0 collective-permute-done.6.refs_8_
  113.1 2.2 %collective-permute-start.8 = (bf16[32,48,128]{2,1,0:T(8,128)(2,1)}, bf16[32,48,128]{2,1,0:T(8,128)(2,1)}, u32[]{:S(2)}, u32[]{:S(2)}) collective-permute-start(bf16[32,48,128]{2,1,0:T(8,128)(2,1)} %collective-permute-done.6.refs_8_), channel_id=1, source_target_pairs={{0,1},{1,0},{2,3},{3,2},{4,5},{5,4},{6,7},{7,6},{8,9},{9,8},{10,11... | collective-permute-start | bytes 1179656 | tf_op jit(solution)/shard_map/ppermute | solution.py:73
  115.4 0.3 convolution_convert_fusion.2
  115.7 0.1 reshape.451
  115.8 0.7 reshape.459
  116.5 0.0 all-to-all-done.2
  116.5 10.7 %all-to-all-start.1 = ((bf16[8,2,256]{2,1,0:T(2,128)(2,1)}), bf16[8,2,256]{2,1,0:T(2,128)(2,1)S(1)}, u32[]{:S(2)}, u32[]{:S(2)}) async-start(bf16[8,2,256]{2,1,0:T(2,128)(2,1)} %reshape.459), calls=%async_computation.1 | async-start | bytes 16384 | tf_op jit(solution)/shard_map/all_to_all | solution.py:147
  127.3 1.0 reshape.453.refs_0_
  128.3 0.0 collective-permute-done.2.refs_4_
  128.3 0.0 collective-permute-done.3.refs_5_
  128.3 0.0 collective-permute-done.4.refs_6_
  128.3 0.0 collective-permute-done.7.refs_9_
  128.3 0.0 collective-permute-done.8.refs_10_
  128.3 5.4 %expert.1 = bf16[64,16,256]{2,1,0:T(8,128)(2,1)} custom-call(bf16[128,2048]{1,0:T(8,128)(2,1)} %reshape.453.refs_0_, bf16[64,48,128]{2,1,0:T(8,128)(2,1)} %copy-done.1, bf16[64,48,128]{2,1,0:T(8,128)(2,1)} %collective-permute-done.refs_2_, bf16[64,48,128]{2,1,0:T(8,128)(2,1)} %collective-permute-done.1.refs_3_, ...), custom_call_target="tpu_custom_call" | custom-call | tf_op jit(solution)/shard_map/expert/pallas_call | solution.py:60
  133.7 4.9 %all-to-all-done.1 = bf16[8,2,256]{2,1,0:T(2,128)(2,1)S(1)} async-done(((bf16[8,2,256]{2,1,0:T(2,128)(2,1)}), bf16[8,2,256]{2,1,0:T(2,128)(2,1)S(1)}, u32[]{:S(2)}, u32[]{:S(2)}) %all-to-all-start.1) | async-done | bytes 8224 | tf_op jit(solution)/shard_map/all_to_all | solution.py:147
  138.7 9.7 %all-to-all-start.3 = ((bf16[64,16,256]{2,1,0:T(8,128)(2,1)}), bf16[64,16,256]{2,1,0:T(8,128)(2,1)S(1)}, u32[]{:S(2)}, u32[]{:S(2)}) async-start(bf16[64,16,256]{2,1,0:T(8,128)(2,1)} %expert.1), calls=%async_computation.3 | async-start | bytes 1048576 | tf_op jit(solution)/shard_map/all_to_all | solution.py:160
  148.3 0.1 reshape.460
  148.4 0.1 broadcast_in_dim.71
  148.5 0.1 broadcast_in_dim.73
  148.6 0.1 convert_element_type.119
  148.7 0.1 broadcast_in_dim.66
  148.8 0.1 broadcast_in_dim.68
  148.9 11.6 %all-to-all-done.3 = bf16[64,16,256]{2,1,0:T(8,128)(2,1)S(1)} async-done(((bf16[64,16,256]{2,1,0:T(8,128)(2,1)}), bf16[64,16,256]{2,1,0:T(8,128)(2,1)S(1)}, u32[]{:S(2)}, u32[]{:S(2)}) %all-to-all-start.3) | async-done | bytes 524320 | tf_op jit(solution)/shard_map/all_to_all | solution.py:160
  160.5 0.6 fusion.1
  161.0 1.3 fusion
  162.4 5.6 %all-to-all-start.4 = ((bf16[8,64,256]{2,1,0:T(8,128)(2,1)}), bf16[8,64,256]{2,1,0:T(8,128)(2,1)}, u32[]{:S(2)}, u32[]{:S(2)}) async-start(bf16[8,64,256]{2,1,0:T(8,128)(2,1)} %bitcast.40), calls=%async_computation.4 | async-start | bytes 524288 | tf_op jit(solution)/shard_map/all_to_all | solution.py:167
  168.0 0.1 fusion.69
  168.2 0.1 pad_maximum_fusion
  168.3 0.9 copy.28
  169.2 1.0 fusion.70
  170.2 1.9 %copy.26 = bf16[1,2048,64]{1,2,0:T(8,128)(2,1)} copy(bf16[1,2048,64]{2,1,0:T(8,128)(2,1)} %bitcast.37) | data formatting | bytes 524288
  172.1 0.9 copy.27
  173.0 15.2 %all-to-all-done.4 = bf16[8,64,256]{2,1,0:T(8,128)(2,1)} async-done(((bf16[8,64,256]{2,1,0:T(8,128)(2,1)}), bf16[8,64,256]{2,1,0:T(8,128)(2,1)}, u32[]{:S(2)}, u32[]{:S(2)}) %all-to-all-start.4) | async-done | bytes 262176 | tf_op jit(solution)/shard_map/all_to_all | solution.py:167
  188.2 2.2 %convolution_convert_fusion = bf16[512,256]{1,0:T(8,128)(2,1)} fusion(bf16[512,256]{1,0:T(8,128)(2,1)} %bitcast.20, s32[512]{0:T(512)S(1)} %bitcast.53, s32[256]{0:T(256)S(1)} %fusion.61), kind=kOutput, calls=%fused_computation.6 | convolution fusion | flops 201916416 | bytes 527360 | tf_op jit(solution)/shard_map/dot_general | solution.py:174
  (38 shorter events, 0.3 us)
Async XLA Ops:
  0.6 23.3 %copy-start = (bf16[512,2048]{1,0:T(8,128)(2,1)S(1)}, bf16[512,2048]{1,0:T(8,128)(2,1)}, u32[]{:S(2)}) copy-start(bf16[512,2048]{1,0:T(8,128)(2,1)} %param.8) | copy-start | bytes 6291460
  0.6 1.7 copy-start.3
  0.7 2.0 %copy-start.4 = (f32[64,32,64]{2,1,0:T(8,128)S(1)}, f32[64,32,64]{2,1,0:T(8,128)}, u32[]{:S(2)}) copy-start(f32[64,32,64]{2,1,0:T(8,128)} %param.11) | copy-start | bytes 1572868
  0.7 2.0 %copy-start.8 = (f32[32]{0:T(128)S(1)}, f32[32]{0:T(128)}, u32[]{:S(2)}) copy-start(f32[32]{0:T(128)} %param.9) | copy-start | bytes 388
  3.0 20.6 %copy-start.5 = (s32[512,2]{0,1:T(2,128)S(1)}, s32[512,2]{0,1:T(2,128)}, u32[]{:S(2)}) copy-start(s32[512,2]{0,1:T(2,128)} %param.13) | copy-start | bytes 12292
  4.3 60.1 %all-to-all-start = ((bf16[64,48,128]{2,1,0:T(8,128)(2,1)}), bf16[64,48,128]{2,1,0:T(8,128)(2,1)S(1)}, u32[]{:S(2)}, u32[]{:S(2)}) async-start(bf16[64,48,128]{2,1,0:T(8,128)(2,1)} %maximum_maximum_fusion), calls=%async_computation | async-start | bytes 1572864 | tf_op jit(solution)/shard_map/all_to_all | solution.py:90
  24.5 55.0 %copy-start.6 = (f32[512,2]{0,1:T(2,128)S(1)}, f32[512,2]{0,1:T(2,128)}, u32[]{:S(2)}) copy-start(f32[512,2]{0,1:T(2,128)} %param.15) | copy-start | bytes 12292
  24.6 85.9 %copy-start.7 = (f32[512]{0:T(512)S(1)}, f32[512]{0:T(512)}, u32[]{:S(2)}) copy-start(f32[512]{0:T(512)} %param.14) | copy-start | bytes 6148
  64.4 63.9 %copy-start.1 = (bf16[64,48,128]{2,1,0:T(8,128)(2,1)}, bf16[64,48,128]{2,1,0:T(8,128)(2,1)S(1)}, u32[]{:S(2)}) copy-start(bf16[64,48,128]{2,1,0:T(8,128)(2,1)S(1)} %all-to-all-done.refs_1_) | copy-start | bytes 2359300
  64.4 52.2 %all-to-all-start.2 = ((bf16[64,32,128]{2,1,0:T(8,128)(2,1)}), bf16[64,32,128]{2,1,0:T(8,128)(2,1)S(1)}, u32[]{:S(2)}, u32[]{:S(2)}) async-start(bf16[64,32,128]{2,1,0:T(8,128)(2,1)} %reshape.452), calls=%async_computation.2 | async-start | bytes 1048576 | tf_op jit(solution)/shard_map/all_to_all | solution.py:123
  73.0 20.9 %collective-permute-start = (bf16[64,48,128]{2,1,0:T(8,128)(2,1)S(1)}, bf16[64,48,128]{2,1,0:T(8,128)(2,1)}, u32[]{:S(2)}, u32[]{:S(2)}) collective-permute-start(bf16[64,48,128]{2,1,0:T(8,128)(2,1)S(1)} %all-to-all-done.refs_1_), channel_id=1, source_target_pairs={{0,2},{2,4},{4,6},{6,0},{1,3},{3,5},{5,7},{7,1},{8,10},{10,12},{12... | collective-permute-start | bytes 2359304 | tf_op jit(solution)/shard_map/ppermute | solution.py:70
  76.1 21.4 %collective-permute-start.1 = (bf16[64,48,128]{2,1,0:T(8,128)(2,1)S(1)}, bf16[64,48,128]{2,1,0:T(8,128)(2,1)}, u32[]{:S(2)}, u32[]{:S(2)}) collective-permute-start(bf16[64,48,128]{2,1,0:T(8,128)(2,1)S(1)} %all-to-all-done.refs_1_), channel_id=1, source_target_pairs={{0,6},{2,0},{4,2},{6,4},{1,7},{3,1},{5,3},{7,5},{8,14},{10,8},{12,... | collective-permute-start | bytes 2359304 | tf_op jit(solution)/shard_map/ppermute | solution.py:70
  79.6 48.7 %collective-permute-start.2 = (bf16[64,48,128]{2,1,0:T(8,128)(2,1)S(1)}, bf16[64,48,128]{2,1,0:T(8,128)(2,1)}, u32[]{:S(2)}, u32[]{:S(2)}) collective-permute-start(bf16[64,48,128]{2,1,0:T(8,128)(2,1)S(1)} %all-to-all-done.refs_1_), channel_id=1, source_target_pairs={{0,1},{1,0},{2,3},{3,2},{4,5},{5,4},{6,7},{7,6},{8,9},{9,8},{10,11... | collective-permute-start | bytes 2359304 | tf_op jit(solution)/shard_map/ppermute | solution.py:73
  95.6 15.1 %collective-permute-start.5 = (bf16[32,48,128]{2,1,0:T(8,128)(2,1)}, bf16[32,48,128]{2,1,0:T(8,128)(2,1)}, u32[]{:S(2)}, u32[]{:S(2)}) collective-permute-start(bf16[32,48,128]{2,1,0:T(8,128)(2,1)} %slice.94), channel_id=1, source_target_pairs={{0,2},{2,4},{4,6},{6,0},{1,3},{3,5},{5,7},{7,1},{8,10},{10,12},{12... | collective-permute-start | bytes 1179656 | tf_op jit(solution)/shard_map/ppermute | solution.py:70
  99.3 13.8 %collective-permute-start.6 = (bf16[32,48,128]{2,1,0:T(8,128)(2,1)}, bf16[32,48,128]{2,1,0:T(8,128)(2,1)}, u32[]{:S(2)}, u32[]{:S(2)}) collective-permute-start(bf16[32,48,128]{2,1,0:T(8,128)(2,1)} %slice.95), channel_id=1, source_target_pairs={{0,6},{2,0},{4,2},{6,4},{1,7},{3,1},{5,3},{7,5},{8,14},{10,8},{12,... | collective-permute-start | bytes 1179656 | tf_op jit(solution)/shard_map/ppermute | solution.py:70
  103.9 24.4 %collective-permute-start.3 = (bf16[64,48,128]{2,1,0:T(8,128)(2,1)}, bf16[64,48,128]{2,1,0:T(8,128)(2,1)}, u32[]{:S(2)}, u32[]{:S(2)}) collective-permute-start(bf16[64,48,128]{2,1,0:T(8,128)(2,1)} %collective-permute-done.refs_2_), channel_id=1, source_target_pairs={{0,1},{1,0},{2,3},{3,2},{4,5},{5,4},{6,7},{7,6},{8,9},{9,8},{10,11... | collective-permute-start | bytes 2359304 | tf_op jit(solution)/shard_map/ppermute | solution.py:73
  108.6 19.7 %collective-permute-start.4 = (bf16[64,48,128]{2,1,0:T(8,128)(2,1)}, bf16[64,48,128]{2,1,0:T(8,128)(2,1)}, u32[]{:S(2)}, u32[]{:S(2)}) collective-permute-start(bf16[64,48,128]{2,1,0:T(8,128)(2,1)} %collective-permute-done.1.refs_3_), channel_id=1, source_target_pairs={{0,1},{1,0},{2,3},{3,2},{4,5},{5,4},{6,7},{7,6},{8,9},{9,8},{10,11... | collective-permute-start | bytes 2359304 | tf_op jit(solution)/shard_map/ppermute | solution.py:73
  110.7 17.6 %collective-permute-start.7 = (bf16[32,48,128]{2,1,0:T(8,128)(2,1)}, bf16[32,48,128]{2,1,0:T(8,128)(2,1)}, u32[]{:S(2)}, u32[]{:S(2)}) collective-permute-start(bf16[32,48,128]{2,1,0:T(8,128)(2,1)} %collective-permute-done.5.refs_7_), channel_id=1, source_target_pairs={{0,1},{1,0},{2,3},{3,2},{4,5},{5,4},{6,7},{7,6},{8,9},{9,8},{10,11... | collective-permute-start | bytes 1179656 | tf_op jit(solution)/shard_map/ppermute | solution.py:73
  113.1 15.2 %collective-permute-start.8 = (bf16[32,48,128]{2,1,0:T(8,128)(2,1)}, bf16[32,48,128]{2,1,0:T(8,128)(2,1)}, u32[]{:S(2)}, u32[]{:S(2)}) collective-permute-start(bf16[32,48,128]{2,1,0:T(8,128)(2,1)} %collective-permute-done.6.refs_8_), channel_id=1, source_target_pairs={{0,1},{1,0},{2,3},{3,2},{4,5},{5,4},{6,7},{7,6},{8,9},{9,8},{10,11... | collective-permute-start | bytes 1179656 | tf_op jit(solution)/shard_map/ppermute | solution.py:73
  116.5 22.1 %all-to-all-start.1 = ((bf16[8,2,256]{2,1,0:T(2,128)(2,1)}), bf16[8,2,256]{2,1,0:T(2,128)(2,1)S(1)}, u32[]{:S(2)}, u32[]{:S(2)}) async-start(bf16[8,2,256]{2,1,0:T(2,128)(2,1)} %reshape.459), calls=%async_computation.1 | async-start | bytes 16384 | tf_op jit(solution)/shard_map/all_to_all | solution.py:147
  138.7 21.8 %all-to-all-start.3 = ((bf16[64,16,256]{2,1,0:T(8,128)(2,1)}), bf16[64,16,256]{2,1,0:T(8,128)(2,1)S(1)}, u32[]{:S(2)}, u32[]{:S(2)}) async-start(bf16[64,16,256]{2,1,0:T(8,128)(2,1)} %expert.1), calls=%async_computation.3 | async-start | bytes 1048576 | tf_op jit(solution)/shard_map/all_to_all | solution.py:160
  161.0 7.0 %copy-start.2 = (bf16[64,48,128]{2,1,0:T(8,128)(2,1)S(1)}, bf16[64,48,128]{2,1,0:T(8,128)(2,1)}, u32[]{:S(2)}) copy-start(bf16[64,48,128]{2,1,0:T(8,128)(2,1)} %copy-done.1) | copy-start | bytes 2359300
  162.4 25.8 %all-to-all-start.4 = ((bf16[8,64,256]{2,1,0:T(8,128)(2,1)}), bf16[8,64,256]{2,1,0:T(8,128)(2,1)}, u32[]{:S(2)}, u32[]{:S(2)}) async-start(bf16[8,64,256]{2,1,0:T(8,128)(2,1)} %bitcast.40), calls=%async_computation.4 | async-start | bytes 524288 | tf_op jit(solution)/shard_map/all_to_all | solution.py:167

commit v2 on v1

--- a/solution.py
+++ b/solution.py
@@ -14,22 +14,15 @@
 F32 = jnp.float32
 
 
-def expert_kernel(*refs):
-    x_ref, shards, out_ref, acc = refs[0], refs[1:-2], refs[-2], refs[-1]
+def expert_kernel(x_ref, *refs):
+    shards, out_ref, acc = refs[:8], refs[8], refs[9]
     x = x_ref[...]
-    groups = [(r,) for r in shards[:6]] + [shards[6:8], shards[8:10]]
-
-    def gate_up(group):
-        return jnp.concatenate([r[:, :32, :].reshape(-1, 128) for r in group], axis=0)
-
-    def down(group):
-        return jnp.concatenate([r[:, 32:, :].reshape(-1, 128) for r in group], axis=0)
-
     lane = lax.broadcasted_iota(jnp.int32, (128, 256), 1) % 128
     low = lane < 64
+    pieces = []
     for k in range(4):
-        a, b = groups[2 * k], groups[2 * k + 1]
-        both = jnp.concatenate([gate_up(a), gate_up(b)], axis=1)
+        pair = shards[2 * k : 2 * k + 2]
+        both = jnp.concatenate([r[:, :32, :].reshape(-1, 128) for r in pair], axis=1)
         pre = jnp.dot(x, both, preferred_element_type=F32)
         other = jnp.concatenate(
             [pltpu.roll(pre[:, :128], 64, 1), pltpu.roll(pre[:, 128:], 64, 1)], axis=1
@@ -37,17 +30,18 @@
         gate = jnp.where(low, pre, other)
         up = jnp.where(low, other, pre)
         hidden = gate / (1.0 + jnp.exp(-gate)) * up
-        stacked = jnp.concatenate(
-            [jnp.where(low, hidden, 0.0), jnp.where(low, 0.0, hidden)], axis=0
-        ).astype(BF)
-        down_pair = jnp.concatenate([down(a), down(b)], axis=1)
-        part = lax.dot_general(
-            stacked, down_pair, (((1,), (1,)), ((), ())), preferred_element_type=F32
+        pieces.append(
+            jnp.concatenate(
+                [jnp.where(low, hidden, 0.0), jnp.where(low, 0.0, hidden)], axis=0
+            ).astype(BF)
         )
-        if k == 0:
-            acc[...] = part
-        else:
-            acc[...] += part
+    down = jnp.concatenate([r[:, 32:, :].reshape(-1, 128) for r in shards], axis=1)
+    acc[...] = lax.dot_general(
+        jnp.concatenate(pieces, axis=1),
+        down,
+        (((1,), (1,)), ((), ())),
+        preferred_element_type=F32,
+    )
     for j in range(8):
         for t in range(8):
             for h in range(2):
@@ -66,20 +60,34 @@
 
 
 def gather_weights(own):
-    def along_x(v, by):
-        return lax.ppermute(v, "x", [(i, (i + by) % 4) for i in range(4)])
+    around = []
+    for i in range(4):
+        around.append((2 * i, 2 * ((i + 1) % 4)))
+        around.append((2 * i + 1, 2 * ((i + 3) % 4) + 1))
+
+    def pass_on(v):
+        return lax.ppermute(v, TP, around)
 
     def swap(v):
         return lax.ppermute(v, "c", [(0, 1), (1, 0)])
 
-    left = along_x(own, 1)
-    right = along_x(own, -1)
+    near = pass_on(own)
     own_c = swap(own)
-    far_a = along_x(left[:32], 1)
-    far_b = along_x(right[32:], -1)
-    left_c, right_c = swap(left), swap(right)
-    far_a_c, far_b_c = swap(far_a), swap(far_b)
-    return (own, left, right, own_c, left_c, right_c, far_a, far_b, far_a_c, far_b_c)
+    other = pass_on(own_c)
+    far = pass_on(near)
+    near_c, other_c, far_c = swap(near), swap(other), swap(far)
+    return own, own_c, near, near_c, other, other_c, far, far_c
+
+
+def trade_facts(facts, shifts):
+    mine = lax.axis_index("g")
+    got = {}
+    for k in shifts:
+        part = lax.dynamic_index_in_dim(facts, (mine + k) & 7, 0, keepdims=False)
+        if k:
+            part = lax.ppermute(part, "g", [(i, (i + k) % 8) for i in range(8)])
+        got[k] = part
+    return got
 
 
 def local(tokens, norm_gain, w_gate, w_up, w_down, route_expert, group_prob, pair_logit):
@@ -117,12 +125,8 @@
         | (send_at(second, rank_second)[None, :] == send_rows)
     ).astype(BF)
     chosen = jnp.dot(pick, tokens, preferred_element_type=F32)
-    normed = (
-        chosen * lax.rsqrt(jnp.mean(chosen * chosen, axis=1, keepdims=True) + EPSILON)
-    ).astype(BF)
-    received = lax.all_to_all(
-        normed.reshape(64, 32, 128), ("l", "y", "g"), split_axis=0, concat_axis=0, tiled=True
-    )
+    mean = jnp.mean(chosen * chosen, axis=1, keepdims=True)
+    normed = (chosen * lax.rsqrt(mean + EPSILON)).astype(BF).reshape(64, 32, 128)
 
     gap = pair_logit[:, 0] - pair_logit[:, 1]
     weight_first = group_prob * jax.nn.sigmoid(gap)
@@ -144,8 +148,16 @@
     to_slot = (slot[:, None] == row_at[None, :]).astype(BF)
     facts = jnp.dot(facts, to_slot, preferred_element_type=F32).astype(BF)
     facts = facts.reshape(8, 8, 64).transpose(1, 0, 2)
-    facts = lax.all_to_all(facts, "g", split_axis=0, concat_axis=0, tiled=True)
-    facts = facts.transpose(1, 0, 2).reshape(8, 512).astype(F32)
+    got = trade_facts(facts, range(2, 7))
+    sent, got = lax.optimization_barrier((normed, got))
+    got.update(trade_facts(facts, (0, 1, 7)))
+    received = lax.all_to_all(
+        sent, ("l", "y", "g"), split_axis=0, concat_axis=0, tiled=True
+    )
+    eight = jnp.arange(8, dtype=jnp.int32)
+    from_group = ((lax.axis_index("g") - eight[:, None]) & 7 == eight[None, :]).astype(BF)
+    facts = jnp.einsum("gk,kfr->fgr", from_group, jnp.stack([got[k] for k in range(8)]), preferred_element_type=F32)
+    facts = facts.reshape(8, 512)
     code = facts[:2].astype(jnp.int32)
     source = row_at // 64
     at = (code // 16 * 8 + code % 16 // 2) * 16 + source[None, :] * 2 + code % 2
@@ -154,9 +166,11 @@
     mix_high = jnp.where(is_first, facts[2][None, :], jnp.where(is_second, facts[3][None, :], 0.0))
     mix_low = jnp.where(is_first, facts[4][None, :], jnp.where(is_second, facts[5][None, :], 0.0))
     mix_high, mix_low = mix_high.astype(BF), mix_low.astype(BF)
-
-    shards = gather_weights(own)
-    outs = expert(received.reshape(128, D), shards)
+    feature = jnp.arange(256, dtype=jnp.int32)
+    lies_at = (feature // 16 % 2) * 128 + feature // 32 * 16 + feature % 16
+    reorder = (lies_at[None, :] == feature[:, None]).astype(BF)
+
+    outs = expert(received.reshape(128, D), gather_weights(own))
     back = lax.all_to_all(outs, IN_GROUP, split_axis=0, concat_axis=0, tiled=True)
     back = back.reshape(1024, 256)
     over_slots = (((0,), (0,)), ((), ()))
@@ -168,9 +182,6 @@
         mixed.reshape(8, 64, 256), "g", split_axis=0, concat_axis=0, tiled=True
     ).reshape(512, 256)
     home = jnp.dot(to_slot, home, preferred_element_type=F32).astype(BF)
-    feature = jnp.arange(256, dtype=jnp.int32)
-    lies_at = (feature // 16 % 2) * 128 + feature // 32 * 16 + feature % 16
-    reorder = (lies_at[None, :] == feature[:, None]).astype(BF)
     home = jnp.dot(home, reorder, preferred_element_type=F32).astype(BF)
     return new_gate, new_up, new_down, home
 

time: 191 us -> 171 us (0.90)
  the two profiles are of different devices: /device:TPU:1 before, /device:TPU:2 now
where the time goes in v2:
time: 171 us; the launch traced here: 170 us
  starting transfers between devices  98 us (57%)
  waiting for transfers between devices  46.5 us (27%)
  local copies, waits for them, and re-layouts  8.22 us (5%)
  matrix products  6.31 us (4%)
  Pallas kernels  5.06 us (3%)
  other arithmetic  4.75 us (3%)
    ppermute x7, starting transfers between devices, trade_facts(): part = lax.ppermute(part, 'g', [(i, (i + k) % 8) for i in range(8)])  42.8 us
    all_to_all x1, starting transfers between devices, local(): own = lax.all_to_all(packed, FS, split_axis=0, concat_axis=0, tiled=True)  18.7 us
    all_to_all x1, waiting for transfers between devices, local(): lax.all_to_all(mixed.reshape(8, 64, 256), 'g', split_axis=0, concat_axis=...  15.8 us
    ppermute x3, waiting for transfers between devices, pass_on(): return lax.ppermute(v, TP, around)  12.3 us
    ppermute x3, starting transfers between devices, pass_on(): return lax.ppermute(v, TP, around)  9.88 us
    all_to_all x1, waiting for transfers between devices, local(): lax.all_to_all(sent, ('l', 'y', 'g'), split_axis=0, concat_axis=0, tiled=...  9.34 us
    ppermute x4, starting transfers between devices, swap(): return lax.ppermute(v, 'c', [(0, 1), (1, 0)])  7.66 us
    all_to_all x1, starting transfers between devices, local(): lax.all_to_all(outs, IN_GROUP, split_axis=0, concat_axis=0, tiled=True)  7.46 us
  transfers between devices with their start and end apart: 18, of which 8 were waited for; matrix products, arithmetic and copies ran while one was open for 7% of the time, Pallas kernels for 0%

profile of v2, /device:TPU:2, one launch (start us, length us, event | category | flops | bytes accessed | tf_op | source)
XLA Modules:
  0.0 170.2 jit_solution(11524678527189922392)
XLA Ops:
  0.6 0.0 copy-start
  0.7 1.5 convert.38
  2.2 0.1 copy-done.3
  2.3 0.3 copy-done.4
  2.7 0.3 multiply_convert_fusion.2
  3.0 0.0 copy-start.5
  3.0 0.0 copy-start.6
  3.0 0.0 copy-start.7
  3.0 1.3 maximum_maximum_fusion
  4.3 18.7 %all-to-all-start = ((bf16[64,48,128]{2,1,0:T(8,128)(2,1)}), bf16[64,48,128]{2,1,0:T(8,128)(2,1)S(1)}, u32[]{:S(2)}, u32[]{:S(2)}) async-start(bf16[64,48,128]{2,1,0:T(8,128)(2,1)} %maximum_maximum_fusion), calls=%async_computation | async-start | bytes 1572864 | tf_op jit(solution)/shard_map/all_to_all | solution.py:98
  23.1 0.3 select_reduce_fusion.2
  23.7 0.3 convolution_convert_fusion.2
  24.0 0.1 reshape.472
  24.2 7.4 %collective-permute-start.1 = (bf16[8,64]{1,0:T(8,128)(2,1)S(1)}, bf16[8,64]{1,0:T(8,128)(2,1)S(1)}, u32[]{:S(2)}, u32[]{:S(2)}) collective-permute-start(bf16[8,64]{1,0:T(8,128)(2,1)S(1)} %bitcast.93), channel_id=1, source_target_pairs={{0,128},{64,192},{128,256},{192,320},{256,384},{320,448},{384,0},{... | collective-permute-start | bytes 3080 | tf_op jit(solution)/shard_map/ppermute | solution.py:88
  31.6 7.4 %collective-permute-start.2 = (bf16[8,64]{1,0:T(8,128)(2,1)S(1)}, bf16[8,64]{1,0:T(8,128)(2,1)S(1)}, u32[]{:S(2)}, u32[]{:S(2)}) collective-permute-start(bf16[8,64]{1,0:T(8,128)(2,1)S(1)} %bitcast.92), channel_id=1, source_target_pairs={{0,192},{64,256},{128,320},{192,384},{256,448},{320,0},{384,64},{4... | collective-permute-start | bytes 3080 | tf_op jit(solution)/shard_map/ppermute | solution.py:88
  39.0 4.1 %collective-permute-start.3 = (bf16[8,64]{1,0:T(8,128)(2,1)S(1)}, bf16[8,64]{1,0:T(8,128)(2,1)S(1)}, u32[]{:S(2)}, u32[]{:S(2)}) collective-permute-start(bf16[8,64]{1,0:T(8,128)(2,1)S(1)} %bitcast.89), channel_id=1, source_target_pairs={{0,256},{64,320},{128,384},{192,448},{256,0},{320,64},{384,128},{4... | collective-permute-start | bytes 3080 | tf_op jit(solution)/shard_map/ppermute | solution.py:88
  43.2 8.7 %collective-permute-start.4 = (bf16[8,64]{1,0:T(8,128)(2,1)S(1)}, bf16[8,64]{1,0:T(8,128)(2,1)S(1)}, u32[]{:S(2)}, u32[]{:S(2)}) collective-permute-start(bf16[8,64]{1,0:T(8,128)(2,1)S(1)} %bitcast.90), channel_id=1, source_target_pairs={{0,320},{64,384},{128,448},{192,0},{256,64},{320,128},{384,192},{4... | collective-permute-start | bytes 3080 | tf_op jit(solution)/shard_map/ppermute | solution.py:88
  51.9 7.2 %collective-permute-start.5 = (bf16[8,64]{1,0:T(8,128)(2,1)S(1)}, bf16[8,64]{1,0:T(8,128)(2,1)S(1)}, u32[]{:S(2)}, u32[]{:S(2)}) collective-permute-start(bf16[8,64]{1,0:T(8,128)(2,1)S(1)} %bitcast.91), channel_id=1, source_target_pairs={{0,384},{64,448},{128,0},{192,64},{256,128},{320,192},{384,256},{4... | collective-permute-start | bytes 3080 | tf_op jit(solution)/shard_map/ppermute | solution.py:88
  59.1 1.4 multiply_reduce_fusion
  60.6 6.7 %all-to-all-done.refs_0_ = bf16[64,48,128]{2,1,0:T(8,128)(2,1)S(1)} async-done(((bf16[64,48,128]{2,1,0:T(8,128)(2,1)}), bf16[64,48,128]{2,1,0:T(8,128)(2,1)S(1)}, u32[]{:S(2)}, u32[]{:S(2)}) %all-to-all-start) | async-done | bytes 786464 | tf_op jit(solution)/shard_map/all_to_all | solution.py:98
  67.3 3.4 %collective-permute-start.8 = (bf16[64,48,128]{2,1,0:T(8,128)(2,1)S(1)}, bf16[64,48,128]{2,1,0:T(8,128)(2,1)}, u32[]{:S(2)}, u32[]{:S(2)}) collective-permute-start(bf16[64,48,128]{2,1,0:T(8,128)(2,1)S(1)} %all-to-all-done.refs_0_), channel_id=1, source_target_pairs={{0,2},{1,7},{2,4},{3,1},{4,6},{5,3},{6,0},{7,5},{8,10},{9,15},{10,... | collective-permute-start | bytes 2359304 | tf_op jit(solution)/shard_map/ppermute | solution.py:69
  70.7 0.0 collective-permute-done.2
  70.7 1.9 %collective-permute-start.7 = (bf16[64,48,128]{2,1,0:T(8,128)(2,1)S(1)}, bf16[64,48,128]{2,1,0:T(8,128)(2,1)}, u32[]{:S(2)}, u32[]{:S(2)}) collective-permute-start(bf16[64,48,128]{2,1,0:T(8,128)(2,1)S(1)} %all-to-all-done.refs_0_), channel_id=1, source_target_pairs={{0,1},{1,0},{2,3},{3,2},{4,5},{5,4},{6,7},{7,6},{8,9},{9,8},{10,11... | collective-permute-start | bytes 2359304 | tf_op jit(solution)/shard_map/ppermute | solution.py:72
  72.6 1.3 multiply_convert_fusion
  73.9 1.0 reshape.473
  75.0 0.0 collective-permute-done.5
  75.0 6.1 %all-to-all-start.1 = ((bf16[64,32,128]{2,1,0:T(8,128)(2,1)}), bf16[64,32,128]{2,1,0:T(8,128)(2,1)S(1)}, u32[]{:S(2)}, u32[]{:S(2)}) async-start(bf16[64,32,128]{2,1,0:T(8,128)(2,1)} %reshape.473), calls=%async_computation.1 | async-start | bytes 1048576 | tf_op jit(solution)/shard_map/all_to_all | solution.py:154
  81.2 0.1 collective-permute-done.8.refs_2_
  81.2 3.4 %collective-permute-start.12 = (bf16[64,48,128]{2,1,0:T(8,128)(2,1)}, bf16[64,48,128]{2,1,0:T(8,128)(2,1)}, u32[]{:S(2)}, u32[]{:S(2)}) collective-permute-start(bf16[64,48,128]{2,1,0:T(8,128)(2,1)} %collective-permute-done.8.refs_2_), channel_id=1, source_target_pairs={{0,2},{1,7},{2,4},{3,1},{4,6},{5,3},{6,0},{7,5},{8,10},{9,15},{10,... | collective-permute-start | bytes 2359304 | tf_op jit(solution)/shard_map/ppermute | solution.py:69
  84.6 0.0 collective-permute-done.7.refs_1_
  84.6 3.1 %collective-permute-start.10 = (bf16[64,48,128]{2,1,0:T(8,128)(2,1)}, bf16[64,48,128]{2,1,0:T(8,128)(2,1)}, u32[]{:S(2)}, u32[]{:S(2)}) collective-permute-start(bf16[64,48,128]{2,1,0:T(8,128)(2,1)} %collective-permute-done.7.refs_1_), channel_id=1, source_target_pairs={{0,2},{1,7},{2,4},{3,1},{4,6},{5,3},{6,0},{7,5},{8,10},{9,15},{10,... | collective-permute-start | bytes 2359304 | tf_op jit(solution)/shard_map/ppermute | solution.py:69
  87.8 1.9 %collective-permute-start.9 = (bf16[64,48,128]{2,1,0:T(8,128)(2,1)}, bf16[64,48,128]{2,1,0:T(8,128)(2,1)}, u32[]{:S(2)}, u32[]{:S(2)}) collective-permute-start(bf16[64,48,128]{2,1,0:T(8,128)(2,1)} %collective-permute-done.8.refs_2_), channel_id=1, source_target_pairs={{0,1},{1,0},{2,3},{3,2},{4,5},{5,4},{6,7},{7,6},{8,9},{9,8},{10,11... | collective-permute-start | bytes 2359304 | tf_op jit(solution)/shard_map/ppermute | solution.py:72
  89.7 5.7 %collective-permute-done.12.refs_6_ = bf16[64,48,128]{2,1,0:T(8,128)(2,1)} collective-permute-done((bf16[64,48,128]{2,1,0:T(8,128)(2,1)}, bf16[64,48,128]{2,1,0:T(8,128)(2,1)}, u32[]{:S(2)}, u32[]{:S(2)}) %collective-permute-start.12) | collective-permute-done | bytes 786464 | tf_op jit(solution)/shard_map/ppermute | solution.py:69
  95.4 1.9 %collective-permute-start.13 = (bf16[64,48,128]{2,1,0:T(8,128)(2,1)}, bf16[64,48,128]{2,1,0:T(8,128)(2,1)}, u32[]{:S(2)}, u32[]{:S(2)}) collective-permute-start(bf16[64,48,128]{2,1,0:T(8,128)(2,1)} %collective-permute-done.12.refs_6_), channel_id=1, source_target_pairs={{0,1},{1,0},{2,3},{3,2},{4,5},{5,4},{6,7},{7,6},{8,9},{9,8},{10,11... | collective-permute-start | bytes 2359304 | tf_op jit(solution)/shard_map/ppermute | solution.py:72
  97.3 6.5 %collective-permute-done.10.refs_4_ = bf16[64,48,128]{2,1,0:T(8,128)(2,1)} collective-permute-done((bf16[64,48,128]{2,1,0:T(8,128)(2,1)}, bf16[64,48,128]{2,1,0:T(8,128)(2,1)}, u32[]{:S(2)}, u32[]{:S(2)}) %collective-permute-start.10) | collective-permute-done | bytes 786464 | tf_op jit(solution)/shard_map/ppermute | solution.py:69
  103.9 1.9 %collective-permute-start.11 = (bf16[64,48,128]{2,1,0:T(8,128)(2,1)}, bf16[64,48,128]{2,1,0:T(8,128)(2,1)}, u32[]{:S(2)}, u32[]{:S(2)}) collective-permute-start(bf16[64,48,128]{2,1,0:T(8,128)(2,1)} %collective-permute-done.10.refs_4_), channel_id=1, source_target_pairs={{0,1},{1,0},{2,3},{3,2},{4,5},{5,4},{6,7},{7,6},{8,9},{9,8},{10,11... | collective-permute-start | bytes 2359304 | tf_op jit(solution)/shard_map/ppermute | solution.py:72
  105.8 9.3 %all-to-all-done.1 = bf16[64,32,128]{2,1,0:T(8,128)(2,1)S(1)} async-done(((bf16[64,32,128]{2,1,0:T(8,128)(2,1)}), bf16[64,32,128]{2,1,0:T(8,128)(2,1)S(1)}, u32[]{:S(2)}, u32[]{:S(2)}) %all-to-all-start.1) | async-done | bytes 524320 | tf_op jit(solution)/shard_map/all_to_all | solution.py:154
  115.1 1.0 reshape.474.x_ref
  116.1 0.0 collective-permute-done.11.refs_5_
  116.2 5.1 %expert.1 = bf16[64,16,256]{2,1,0:T(8,128)(2,1)} custom-call(bf16[128,2048]{1,0:T(8,128)(2,1)} %reshape.474.x_ref, bf16[64,48,128]{2,1,0:T(8,128)(2,1)} %copy-done.1, bf16[64,48,128]{2,1,0:T(8,128)(2,1)} %collective-permute-done.7.refs_1_, bf16[64,48,128]{2,1,0:T(8,128)(2,1)} %collective-permute-done.8.refs_2_, ...), custom_call_target="tpu_custom_call" | custom-call | tf_op jit(solution)/shard_map/expert/pallas_call | solution.py:54
  121.2 7.5 %all-to-all-start.2 = ((bf16[64,16,256]{2,1,0:T(8,128)(2,1)}), bf16[64,16,256]{2,1,0:T(8,128)(2,1)S(1)}, u32[]{:S(2)}, u32[]{:S(2)}) async-start(bf16[64,16,256]{2,1,0:T(8,128)(2,1)} %expert.1), calls=%async_computation.2 | async-start | bytes 1048576 | tf_op jit(solution)/shard_map/all_to_all | solution.py:174
  128.7 2.4 %collective-permute-start = (bf16[8,64]{1,0:T(8,128)(2,1)S(1)}, bf16[8,64]{1,0:T(8,128)(2,1)S(1)}, u32[]{:S(2)}, u32[]{:S(2)}) collective-permute-start(bf16[8,64]{1,0:T(8,128)(2,1)S(1)} %bitcast.94), channel_id=1, source_target_pairs={{0,64},{64,128},{128,192},{192,256},{256,320},{320,384},{384,448},... | collective-permute-start | bytes 3080 | tf_op jit(solution)/shard_map/ppermute | solution.py:88
  131.1 5.6 %collective-permute-start.6 = (bf16[8,64]{1,0:T(8,128)(2,1)S(1)}, bf16[8,64]{1,0:T(8,128)(2,1)S(1)}, u32[]{:S(2)}, u32[]{:S(2)}) collective-permute-start(bf16[8,64]{1,0:T(8,128)(2,1)S(1)} %bitcast.96), channel_id=1, source_target_pairs={{0,448},{64,0},{128,64},{192,128},{256,192},{320,256},{384,320},{4... | collective-permute-start | bytes 3080 | tf_op jit(solution)/shard_map/ppermute | solution.py:88
  136.8 0.0 collective-permute-done
  136.8 1.2 collective-permute-done.6
  138.0 0.1 stack.63
  138.0 0.2 convolution_bitcast_fusion
  138.2 0.1 convert_element_type.112
  138.3 0.1 broadcast_in_dim.73
  138.4 0.1 broadcast_in_dim.75
  138.5 0.1 broadcast_in_dim.68
  138.6 0.1 broadcast_in_dim.70
  138.7 1.1 all-to-all-done.2
  139.8 0.6 fusion.1
  140.4 1.3 fusion
  141.8 5.4 %all-to-all-start.3 = ((bf16[8,64,256]{2,1,0:T(8,128)(2,1)}), bf16[8,64,256]{2,1,0:T(8,128)(2,1)}, u32[]{:S(2)}, u32[]{:S(2)}) async-start(bf16[8,64,256]{2,1,0:T(8,128)(2,1)} %bitcast.71), calls=%async_computation.3 | async-start | bytes 524288 | tf_op jit(solution)/shard_map/all_to_all | solution.py:181
  147.2 0.1 fusion.72
  147.3 0.1 pad_maximum_fusion
  147.5 0.9 copy.31
  148.4 1.0 fusion.73
  149.3 1.9 %copy.29 = bf16[1,2048,64]{1,2,0:T(8,128)(2,1)} copy(bf16[1,2048,64]{2,1,0:T(8,128)(2,1)} %bitcast.68) | data formatting | bytes 524288
  151.3 0.9 copy.30
  152.2 15.8 %all-to-all-done.3 = bf16[8,64,256]{2,1,0:T(8,128)(2,1)} async-done(((bf16[8,64,256]{2,1,0:T(8,128)(2,1)}), bf16[8,64,256]{2,1,0:T(8,128)(2,1)}, u32[]{:S(2)}, u32[]{:S(2)}) %all-to-all-start.3) | async-done | bytes 262176 | tf_op jit(solution)/shard_map/all_to_all | solution.py:181
  168.0 2.2 %convolution_convert_fusion = bf16[512,256]{1,0:T(8,128)(2,1)} fusion(bf16[512,256]{1,0:T(8,128)(2,1)} %bitcast.35, s32[512]{0:T(512)S(1)} %bitcast.83, s32[256]{0:T(256)S(1)} %fusion.64), kind=kOutput, calls=%fused_computation.6 | convolution fusion | flops 201916416 | bytes 527360 | tf_op jit(solution)/shard_map/dot_general | solution.py:185
  (58 shorter events, 0.5 us)
Async XLA Ops:
  0.6 58.5 %copy-start = (bf16[512,2048]{1,0:T(8,128)(2,1)S(1)}, bf16[512,2048]{1,0:T(8,128)(2,1)}, u32[]{:S(2)}) copy-start(bf16[512,2048]{1,0:T(8,128)(2,1)} %param.8) | copy-start | bytes 6291460
  0.6 1.7 copy-start.3
  0.7 2.0 %copy-start.4 = (f32[64,32,64]{2,1,0:T(8,128)S(1)}, f32[64,32,64]{2,1,0:T(8,128)}, u32[]{:S(2)}) copy-start(f32[64,32,64]{2,1,0:T(8,128)} %param.11) | copy-start | bytes 1572868
  0.7 2.0 %copy-start.8 = (f32[32]{0:T(128)S(1)}, f32[32]{0:T(128)}, u32[]{:S(2)}) copy-start(f32[32]{0:T(128)} %param.9) | copy-start | bytes 388
  3.0 20.2 %copy-start.5 = (s32[512,2]{0,1:T(2,128)S(1)}, s32[512,2]{0,1:T(2,128)}, u32[]{:S(2)}) copy-start(s32[512,2]{0,1:T(2,128)} %param.13) | copy-start | bytes 12292
  3.0 20.5 %copy-start.6 = (f32[512,2]{0,1:T(2,128)S(1)}, f32[512,2]{0,1:T(2,128)}, u32[]{:S(2)}) copy-start(f32[512,2]{0,1:T(2,128)} %param.15) | copy-start | bytes 12292
  3.0 20.5 %copy-start.7 = (f32[512]{0:T(512)S(1)}, f32[512]{0:T(512)}, u32[]{:S(2)}) copy-start(f32[512]{0:T(512)} %param.14) | copy-start | bytes 6148
  4.3 62.9 %all-to-all-start = ((bf16[64,48,128]{2,1,0:T(8,128)(2,1)}), bf16[64,48,128]{2,1,0:T(8,128)(2,1)S(1)}, u32[]{:S(2)}, u32[]{:S(2)}) async-start(bf16[64,48,128]{2,1,0:T(8,128)(2,1)} %maximum_maximum_fusion), calls=%async_computation | async-start | bytes 1572864 | tf_op jit(solution)/shard_map/all_to_all | solution.py:98
  24.2 36.4 %collective-permute-start.1 = (bf16[8,64]{1,0:T(8,128)(2,1)S(1)}, bf16[8,64]{1,0:T(8,128)(2,1)S(1)}, u32[]{:S(2)}, u32[]{:S(2)}) collective-permute-start(bf16[8,64]{1,0:T(8,128)(2,1)S(1)} %bitcast.93), channel_id=1, source_target_pairs={{0,128},{64,192},{128,256},{192,320},{256,384},{320,448},{384,0},{... | collective-permute-start | bytes 3080 | tf_op jit(solution)/shard_map/ppermute | solution.py:88
  31.6 39.1 %collective-permute-start.2 = (bf16[8,64]{1,0:T(8,128)(2,1)S(1)}, bf16[8,64]{1,0:T(8,128)(2,1)S(1)}, u32[]{:S(2)}, u32[]{:S(2)}) collective-permute-start(bf16[8,64]{1,0:T(8,128)(2,1)S(1)} %bitcast.92), channel_id=1, source_target_pairs={{0,192},{64,256},{128,320},{192,384},{256,448},{320,0},{384,64},{4... | collective-permute-start | bytes 3080 | tf_op jit(solution)/shard_map/ppermute | solution.py:88
  39.0 36.0 %collective-permute-start.3 = (bf16[8,64]{1,0:T(8,128)(2,1)S(1)}, bf16[8,64]{1,0:T(8,128)(2,1)S(1)}, u32[]{:S(2)}, u32[]{:S(2)}) collective-permute-start(bf16[8,64]{1,0:T(8,128)(2,1)S(1)} %bitcast.89), channel_id=1, source_target_pairs={{0,256},{64,320},{128,384},{192,448},{256,0},{320,64},{384,128},{4... | collective-permute-start | bytes 3080 | tf_op jit(solution)/shard_map/ppermute | solution.py:88
  43.2 31.8 %collective-permute-start.4 = (bf16[8,64]{1,0:T(8,128)(2,1)S(1)}, bf16[8,64]{1,0:T(8,128)(2,1)S(1)}, u32[]{:S(2)}, u32[]{:S(2)}) collective-permute-start(bf16[8,64]{1,0:T(8,128)(2,1)S(1)} %bitcast.90), channel_id=1, source_target_pairs={{0,320},{64,384},{128,448},{192,0},{256,64},{320,128},{384,192},{4... | collective-permute-start | bytes 3080 | tf_op jit(solution)/shard_map/ppermute | solution.py:88
  51.9 23.1 %collective-permute-start.5 = (bf16[8,64]{1,0:T(8,128)(2,1)S(1)}, bf16[8,64]{1,0:T(8,128)(2,1)S(1)}, u32[]{:S(2)}, u32[]{:S(2)}) collective-permute-start(bf16[8,64]{1,0:T(8,128)(2,1)S(1)} %bitcast.91), channel_id=1, source_target_pairs={{0,384},{64,448},{128,0},{192,64},{256,128},{320,192},{384,256},{4... | collective-permute-start | bytes 3080 | tf_op jit(solution)/shard_map/ppermute | solution.py:88
  67.3 48.9 %copy-start.1 = (bf16[64,48,128]{2,1,0:T(8,128)(2,1)}, bf16[64,48,128]{2,1,0:T(8,128)(2,1)S(1)}, u32[]{:S(2)}) copy-start(bf16[64,48,128]{2,1,0:T(8,128)(2,1)S(1)} %all-to-all-done.refs_0_) | copy-start | bytes 2359300
  67.3 14.0 %collective-permute-start.8 = (bf16[64,48,128]{2,1,0:T(8,128)(2,1)S(1)}, bf16[64,48,128]{2,1,0:T(8,128)(2,1)}, u32[]{:S(2)}, u32[]{:S(2)}) collective-permute-start(bf16[64,48,128]{2,1,0:T(8,128)(2,1)S(1)} %all-to-all-done.refs_0_), channel_id=1, source_target_pairs={{0,2},{1,7},{2,4},{3,1},{4,6},{5,3},{6,0},{7,5},{8,10},{9,15},{10,... | collective-permute-start | bytes 2359304 | tf_op jit(solution)/shard_map/ppermute | solution.py:69
  70.7 14.0 %collective-permute-start.7 = (bf16[64,48,128]{2,1,0:T(8,128)(2,1)S(1)}, bf16[64,48,128]{2,1,0:T(8,128)(2,1)}, u32[]{:S(2)}, u32[]{:S(2)}) collective-permute-start(bf16[64,48,128]{2,1,0:T(8,128)(2,1)S(1)} %all-to-all-done.refs_0_), channel_id=1, source_target_pairs={{0,1},{1,0},{2,3},{3,2},{4,5},{5,4},{6,7},{7,6},{8,9},{9,8},{10,11... | collective-permute-start | bytes 2359304 | tf_op jit(solution)/shard_map/ppermute | solution.py:72
  75.0 40.1 %all-to-all-start.1 = ((bf16[64,32,128]{2,1,0:T(8,128)(2,1)}), bf16[64,32,128]{2,1,0:T(8,128)(2,1)S(1)}, u32[]{:S(2)}, u32[]{:S(2)}) async-start(bf16[64,32,128]{2,1,0:T(8,128)(2,1)} %reshape.473), calls=%async_computation.1 | async-start | bytes 1048576 | tf_op jit(solution)/shard_map/all_to_all | solution.py:154
  81.2 14.2 %collective-permute-start.12 = (bf16[64,48,128]{2,1,0:T(8,128)(2,1)}, bf16[64,48,128]{2,1,0:T(8,128)(2,1)}, u32[]{:S(2)}, u32[]{:S(2)}) collective-permute-start(bf16[64,48,128]{2,1,0:T(8,128)(2,1)} %collective-permute-done.8.refs_2_), channel_id=1, source_target_pairs={{0,2},{1,7},{2,4},{3,1},{4,6},{5,3},{6,0},{7,5},{8,10},{9,15},{10,... | collective-permute-start | bytes 2359304 | tf_op jit(solution)/shard_map/ppermute | solution.py:69
  84.6 19.2 %collective-permute-start.10 = (bf16[64,48,128]{2,1,0:T(8,128)(2,1)}, bf16[64,48,128]{2,1,0:T(8,128)(2,1)}, u32[]{:S(2)}, u32[]{:S(2)}) collective-permute-start(bf16[64,48,128]{2,1,0:T(8,128)(2,1)} %collective-permute-done.7.refs_1_), channel_id=1, source_target_pairs={{0,2},{1,7},{2,4},{3,1},{4,6},{5,3},{6,0},{7,5},{8,10},{9,15},{10,... | collective-permute-start | bytes 2359304 | tf_op jit(solution)/shard_map/ppermute | solution.py:69
  87.8 28.4 %collective-permute-start.9 = (bf16[64,48,128]{2,1,0:T(8,128)(2,1)}, bf16[64,48,128]{2,1,0:T(8,128)(2,1)}, u32[]{:S(2)}, u32[]{:S(2)}) collective-permute-start(bf16[64,48,128]{2,1,0:T(8,128)(2,1)} %collective-permute-done.8.refs_2_), channel_id=1, source_target_pairs={{0,1},{1,0},{2,3},{3,2},{4,5},{5,4},{6,7},{7,6},{8,9},{9,8},{10,11... | collective-permute-start | bytes 2359304 | tf_op jit(solution)/shard_map/ppermute | solution.py:72
  95.4 20.7 %collective-permute-start.13 = (bf16[64,48,128]{2,1,0:T(8,128)(2,1)}, bf16[64,48,128]{2,1,0:T(8,128)(2,1)}, u32[]{:S(2)}, u32[]{:S(2)}) collective-permute-start(bf16[64,48,128]{2,1,0:T(8,128)(2,1)} %collective-permute-done.12.refs_6_), channel_id=1, source_target_pairs={{0,1},{1,0},{2,3},{3,2},{4,5},{5,4},{6,7},{7,6},{8,9},{9,8},{10,11... | collective-permute-start | bytes 2359304 | tf_op jit(solution)/shard_map/ppermute | solution.py:72
  103.9 12.3 %collective-permute-start.11 = (bf16[64,48,128]{2,1,0:T(8,128)(2,1)}, bf16[64,48,128]{2,1,0:T(8,128)(2,1)}, u32[]{:S(2)}, u32[]{:S(2)}) collective-permute-start(bf16[64,48,128]{2,1,0:T(8,128)(2,1)} %collective-permute-done.10.refs_4_), channel_id=1, source_target_pairs={{0,1},{1,0},{2,3},{3,2},{4,5},{5,4},{6,7},{7,6},{8,9},{9,8},{10,11... | collective-permute-start | bytes 2359304 | tf_op jit(solution)/shard_map/ppermute | solution.py:72
  121.2 18.6 %all-to-all-start.2 = ((bf16[64,16,256]{2,1,0:T(8,128)(2,1)}), bf16[64,16,256]{2,1,0:T(8,128)(2,1)S(1)}, u32[]{:S(2)}, u32[]{:S(2)}) async-start(bf16[64,16,256]{2,1,0:T(8,128)(2,1)} %expert.1), calls=%async_computation.2 | async-start | bytes 1048576 | tf_op jit(solution)/shard_map/all_to_all | solution.py:174
  128.7 8.1 %collective-permute-start = (bf16[8,64]{1,0:T(8,128)(2,1)S(1)}, bf16[8,64]{1,0:T(8,128)(2,1)S(1)}, u32[]{:S(2)}, u32[]{:S(2)}) collective-permute-start(bf16[8,64]{1,0:T(8,128)(2,1)S(1)} %bitcast.94), channel_id=1, source_target_pairs={{0,64},{64,128},{128,192},{192,256},{256,320},{320,384},{384,448},... | collective-permute-start | bytes 3080 | tf_op jit(solution)/shard_map/ppermute | solution.py:88
  131.1 6.9 %collective-permute-start.6 = (bf16[8,64]{1,0:T(8,128)(2,1)S(1)}, bf16[8,64]{1,0:T(8,128)(2,1)S(1)}, u32[]{:S(2)}, u32[]{:S(2)}) collective-permute-start(bf16[8,64]{1,0:T(8,128)(2,1)S(1)} %bitcast.96), channel_id=1, source_target_pairs={{0,448},{64,0},{128,64},{192,128},{256,192},{320,256},{384,320},{4... | collective-permute-start | bytes 3080 | tf_op jit(solution)/shard_map/ppermute | solution.py:88
  140.4 6.8 %copy-start.2 = (bf16[64,48,128]{2,1,0:T(8,128)(2,1)S(1)}, bf16[64,48,128]{2,1,0:T(8,128)(2,1)}, u32[]{:S(2)}) copy-start(bf16[64,48,128]{2,1,0:T(8,128)(2,1)} %copy-done.1) | copy-start | bytes 2359300
  141.8 26.2 %all-to-all-start.3 = ((bf16[8,64,256]{2,1,0:T(8,128)(2,1)}), bf16[8,64,256]{2,1,0:T(8,128)(2,1)}, u32[]{:S(2)}, u32[]{:S(2)}) async-start(bf16[8,64,256]{2,1,0:T(8,128)(2,1)} %bitcast.71), calls=%async_computation.3 | async-start | bytes 524288 | tf_op jit(solution)/shard_map/all_to_all | solution.py:181

commit v3 on v2

--- a/solution.py
+++ b/solution.py
@@ -12,6 +12,37 @@
 IN_GROUP = ("l", "y", "x", "c")
 BF = jnp.bfloat16
 F32 = jnp.float32
+
+
+def pack_kernel(gain_ref, gate_ref, up_ref, down_ref, out_ref):
+    along = jnp.broadcast_to(gain_ref[...], (32, 32))
+    diagonal = lax.broadcasted_iota(jnp.int32, (32, 32), 0) == lax.broadcasted_iota(
+        jnp.int32, (32, 32), 1
+    )
+    gain = jnp.sum(jnp.where(diagonal, along, 0.0), axis=1, keepdims=True)[None]
+    out_ref[:, :32, :64] = (gate_ref[...] * gain).astype(BF)
+    out_ref[:, :32, 64:] = (up_ref[...] * gain).astype(BF)
+    out_ref[:, 32:, :64] = down_ref[:, :16, :].astype(BF)
+    out_ref[:, 32:, 64:] = down_ref[:, 16:, :].astype(BF)
+
+
+def pack(norm_gain, w_gate, w_up, w_down):
+    return pl.pallas_call(
+        pack_kernel, out_shape=jax.ShapeDtypeStruct((64, 48, 128), BF), name="pack"
+    )(norm_gain.reshape(1, 32), w_gate, w_up, w_down)
+
+
+def home_kernel(slot_ref, back_ref, out_ref):
+    row = lax.broadcasted_iota(jnp.int32, (512, 512), 0)
+    at_slot = (row == slot_ref[...]).astype(F32).astype(BF)
+    rows = lax.dot_general(
+        at_slot, back_ref[...], (((0,), (0,)), ((), ())), preferred_element_type=F32
+    ).astype(BF)
+    lies = lax.broadcasted_iota(jnp.int32, (256, 256), 0)
+    feature = lax.broadcasted_iota(jnp.int32, (256, 256), 1)
+    lies_at = ((feature >> 4) & 1) * 128 + (feature >> 5) * 16 + (feature & 15)
+    reorder = (lies == lies_at).astype(F32).astype(BF)
+    out_ref[...] = jnp.dot(rows, reorder, preferred_element_type=F32).astype(BF)
 
 
 def expert_kernel(x_ref, *refs):
@@ -91,10 +122,7 @@
 
 
 def local(tokens, norm_gain, w_gate, w_up, w_down, route_expert, group_prob, pair_logit):
-    scale = norm_gain[None, :, None]
-    gate_up = jnp.concatenate([w_gate * scale, w_up * scale], axis=2).astype(BF)
-    down = jnp.concatenate([w_down[:, :16], w_down[:, 16:]], axis=2).astype(BF)
-    packed = jnp.concatenate([gate_up, down], axis=1)
+    packed = pack(norm_gain, w_gate, w_up, w_down)
     own = lax.all_to_all(packed, FS, split_axis=0, concat_axis=0, tiled=True)
     new_gate = own[:, :32, :64].reshape(1, D, 64)
     new_up = own[:, :32, 64:].reshape(1, D, 64)
@@ -131,16 +159,14 @@
     gap = pair_logit[:, 0] - pair_logit[:, 1]
     weight_first = group_prob * jax.nn.sigmoid(gap)
     weight_second = group_prob * jax.nn.sigmoid(-gap)
-    high_first = lax.reduce_precision(weight_first, 8, 7)
-    high_second = lax.reduce_precision(weight_second, 8, 7)
     facts = jnp.stack(
         [
             ((first % 8) * 16 + rank_first).astype(F32),
             ((second % 8) * 16 + rank_second).astype(F32),
-            high_first,
-            high_second,
-            weight_first - high_first,
-            weight_second - high_second,
+            weight_first,
+            weight_second,
+            jnp.zeros_like(gap),
+            jnp.zeros_like(gap),
             jnp.zeros_like(gap),
             jnp.zeros_like(gap),
         ]
@@ -148,9 +174,9 @@
     to_slot = (slot[:, None] == row_at[None, :]).astype(BF)
     facts = jnp.dot(facts, to_slot, preferred_element_type=F32).astype(BF)
     facts = facts.reshape(8, 8, 64).transpose(1, 0, 2)
-    got = trade_facts(facts, range(2, 7))
+    got = trade_facts(facts, range(1, 7))
     sent, got = lax.optimization_barrier((normed, got))
-    got.update(trade_facts(facts, (0, 1, 7)))
+    got.update(trade_facts(facts, (0, 7)))
     received = lax.all_to_all(
         sent, ("l", "y", "g"), split_axis=0, concat_axis=0, tiled=True
     )
@@ -163,26 +189,19 @@
     at = (code // 16 * 8 + code % 16 // 2) * 16 + source[None, :] * 2 + code % 2
     slots = jnp.arange(1024, dtype=jnp.int32)[:, None]
     is_first, is_second = at[0][None, :] == slots, at[1][None, :] == slots
-    mix_high = jnp.where(is_first, facts[2][None, :], jnp.where(is_second, facts[3][None, :], 0.0))
-    mix_low = jnp.where(is_first, facts[4][None, :], jnp.where(is_second, facts[5][None, :], 0.0))
-    mix_high, mix_low = mix_high.astype(BF), mix_low.astype(BF)
-    feature = jnp.arange(256, dtype=jnp.int32)
-    lies_at = (feature // 16 % 2) * 128 + feature // 32 * 16 + feature % 16
-    reorder = (lies_at[None, :] == feature[:, None]).astype(BF)
-
+    mix = jnp.where(is_first, facts[2][None, :], jnp.where(is_second, facts[3][None, :], 0.0))
+    mix = mix.astype(BF)
     outs = expert(received.reshape(128, D), gather_weights(own))
     back = lax.all_to_all(outs, IN_GROUP, split_axis=0, concat_axis=0, tiled=True)
     back = back.reshape(1024, 256)
     over_slots = (((0,), (0,)), ((), ()))
-    mixed = (
-        lax.dot_general(mix_high, back, over_slots, preferred_element_type=F32)
-        + lax.dot_general(mix_low, back, over_slots, preferred_element_type=F32)
-    ).astype(BF)
+    mixed = lax.dot_general(mix, back, over_slots, preferred_element_type=F32).astype(BF)
     home = lax.all_to_all(
         mixed.reshape(8, 64, 256), "g", split_axis=0, concat_axis=0, tiled=True
     ).reshape(512, 256)
-    home = jnp.dot(to_slot, home, preferred_element_type=F32).astype(BF)
-    home = jnp.dot(home, reorder, preferred_element_type=F32).astype(BF)
+    home = pl.pallas_call(
+        home_kernel, out_shape=jax.ShapeDtypeStruct((512, 256), BF), name="home"
+    )(slot.reshape(1, 512), home)
     return new_gate, new_up, new_down, home
 
 

time: 171 us -> 174 us (1.018)
  the two profiles are of different devices: /device:TPU:2 before, /device:TPU:1 now
where the time goes in v3:
time: 174 us; the launch traced here: 173 us
  starting transfers between devices  105 us (60%)
  waiting for transfers between devices  42.6 us (24%)
  Pallas kernels  10.7 us (6%)
  local copies, waits for them, and re-layouts  7.56 us (4%)
  matrix products  3.6 us (2%)
  other arithmetic  2.21 us (1%)
    ppermute x7, starting transfers between devices, trade_facts(): part = lax.ppermute(part, 'g', [(i, (i + k) % 8) for i in range(8)])  37 us
    all_to_all x1, starting transfers between devices, local(): own = lax.all_to_all(packed, FS, split_axis=0, concat_axis=0, tiled=True)  19.4 us
    ppermute x4, starting transfers between devices, swap(): return lax.ppermute(v, 'c', [(0, 1), (1, 0)])  15.9 us
    all_to_all x1, waiting for transfers between devices, local(): lax.all_to_all(mixed.reshape(8, 64, 256), 'g', split_axis=0, concat_axis=...  15.8 us
    ppermute x3, starting transfers between devices, pass_on(): return lax.ppermute(v, TP, around)  10.9 us
    all_to_all x1, starting transfers between devices, local(): lax.all_to_all(outs, IN_GROUP, split_axis=0, concat_axis=0, tiled=True)  9.79 us
    ppermute x3, waiting for transfers between devices, pass_on(): return lax.ppermute(v, TP, around)  8.77 us
    all_to_all x1, starting transfers between devices, local(): lax.all_to_all(sent, ('l', 'y', 'g'), split_axis=0, concat_axis=0, tiled=...  7.9 us
  transfers between devices with their start and end apart: 18, of which 8 were waited for; matrix products, arithmetic and copies ran while one was open for 7% of the time, Pallas kernels for 0%

profile of v3, /device:TPU:1, one launch (start us, length us, event | category | flops | bytes accessed | tf_op | source)
XLA Modules:
  0.0 172.9 jit_solution(14039816074462481878)
XLA Ops:
  0.6 0.0 copy-start
  0.6 0.0 copy-start.3
  0.7 3.5 %pack.1 = bf16[64,48,128]{2,1,0:T(8,128)(2,1)} custom-call(f32[1,32]{1,0:T(1,128)} %bitcast.109, f32[64,32,64]{2,1,0:T(8,128)} %gate_ref.1, f32[64,32,64]{2,1,0:T(8,128)} %up_ref.1, f32[64,32,64]{2,1,0:T(8,128)} %down_ref.1), custom_call_target="tpu_custom_call" | custom-call | tf_op jit(solution)/shard_map/pack/pallas_call | solution.py:30
  4.1 19.4 %all-to-all-start = ((bf16[64,48,128]{2,1,0:T(8,128)(2,1)}), bf16[64,48,128]{2,1,0:T(8,128)(2,1)S(1)}, u32[]{:S(2)}, u32[]{:S(2)}) async-start(bf16[64,48,128]{2,1,0:T(8,128)(2,1)} %pack.1), calls=%async_computation | async-start | bytes 1572864 | tf_op jit(solution)/shard_map/all_to_all | solution.py:126
  23.6 0.0 copy-done.3
  23.6 0.3 select_reduce_fusion.1
  23.9 0.0 copy-done.4
  24.1 0.3 convolution_convert_fusion.1
  24.5 0.1 reshape.479
  24.6 3.8 %collective-permute-start = (bf16[8,64]{1,0:T(8,128)(2,1)S(1)}, bf16[8,64]{1,0:T(8,128)(2,1)S(1)}, u32[]{:S(2)}, u32[]{:S(2)}) collective-permute-start(bf16[8,64]{1,0:T(8,128)(2,1)S(1)} %bitcast.102), channel_id=1, source_target_pairs={{0,64},{64,128},{128,192},{192,256},{256,320},{320,384},{384,448},... | collective-permute-start | bytes 3080 | tf_op jit(solution)/shard_map/ppermute | solution.py:119
  28.5 7.0 %collective-permute-start.1 = (bf16[8,64]{1,0:T(8,128)(2,1)S(1)}, bf16[8,64]{1,0:T(8,128)(2,1)S(1)}, u32[]{:S(2)}, u32[]{:S(2)}) collective-permute-start(bf16[8,64]{1,0:T(8,128)(2,1)S(1)} %bitcast.101), channel_id=1, source_target_pairs={{0,128},{64,192},{128,256},{192,320},{256,384},{320,448},{384,0},{... | collective-permute-start | bytes 3080 | tf_op jit(solution)/shard_map/ppermute | solution.py:119
  35.5 5.4 %collective-permute-start.2 = (bf16[8,64]{1,0:T(8,128)(2,1)S(1)}, bf16[8,64]{1,0:T(8,128)(2,1)S(1)}, u32[]{:S(2)}, u32[]{:S(2)}) collective-permute-start(bf16[8,64]{1,0:T(8,128)(2,1)S(1)} %bitcast.100), channel_id=1, source_target_pairs={{0,192},{64,256},{128,320},{192,384},{256,448},{320,0},{384,64},{4... | collective-permute-start | bytes 3080 | tf_op jit(solution)/shard_map/ppermute | solution.py:119
  40.9 6.8 %collective-permute-start.3 = (bf16[8,64]{1,0:T(8,128)(2,1)S(1)}, bf16[8,64]{1,0:T(8,128)(2,1)S(1)}, u32[]{:S(2)}, u32[]{:S(2)}) collective-permute-start(bf16[8,64]{1,0:T(8,128)(2,1)S(1)} %bitcast.98), channel_id=1, source_target_pairs={{0,256},{64,320},{128,384},{192,448},{256,0},{320,64},{384,128},{4... | collective-permute-start | bytes 3080 | tf_op jit(solution)/shard_map/ppermute | solution.py:119
  47.7 5.5 %collective-permute-start.4 = (bf16[8,64]{1,0:T(8,128)(2,1)S(1)}, bf16[8,64]{1,0:T(8,128)(2,1)S(1)}, u32[]{:S(2)}, u32[]{:S(2)}) collective-permute-start(bf16[8,64]{1,0:T(8,128)(2,1)S(1)} %bitcast.99), channel_id=1, source_target_pairs={{0,320},{64,384},{128,448},{192,0},{256,64},{320,128},{384,192},{4... | collective-permute-start | bytes 3080 | tf_op jit(solution)/shard_map/ppermute | solution.py:119
  53.2 0.0 copy-done
  53.2 1.4 multiply_reduce_fusion
  54.7 1.5 collective-permute-done
  56.1 6.6 %collective-permute-start.5 = (bf16[8,64]{1,0:T(8,128)(2,1)S(1)}, bf16[8,64]{1,0:T(8,128)(2,1)S(1)}, u32[]{:S(2)}, u32[]{:S(2)}) collective-permute-start(bf16[8,64]{1,0:T(8,128)(2,1)S(1)} %bitcast.103), channel_id=1, source_target_pairs={{0,384},{64,448},{128,0},{192,64},{256,128},{320,192},{384,256},{4... | collective-permute-start | bytes 3080 | tf_op jit(solution)/shard_map/ppermute | solution.py:119
  62.8 0.0 collective-permute-done.1
  62.8 1.6 all-to-all-done.refs_0_
  64.4 4.4 %collective-permute-start.8 = (bf16[64,48,128]{2,1,0:T(8,128)(2,1)S(1)}, bf16[64,48,128]{2,1,0:T(8,128)(2,1)}, u32[]{:S(2)}, u32[]{:S(2)}) collective-permute-start(bf16[64,48,128]{2,1,0:T(8,128)(2,1)S(1)} %all-to-all-done.refs_0_), channel_id=1, source_target_pairs={{0,2},{1,7},{2,4},{3,1},{4,6},{5,3},{6,0},{7,5},{8,10},{9,15},{10,... | collective-permute-start | bytes 2359304 | tf_op jit(solution)/shard_map/ppermute | solution.py:100
  68.8 0.0 collective-permute-done.2
  68.8 5.3 %collective-permute-start.7 = (bf16[64,48,128]{2,1,0:T(8,128)(2,1)S(1)}, bf16[64,48,128]{2,1,0:T(8,128)(2,1)}, u32[]{:S(2)}, u32[]{:S(2)}) collective-permute-start(bf16[64,48,128]{2,1,0:T(8,128)(2,1)S(1)} %all-to-all-done.refs_0_), channel_id=1, source_target_pairs={{0,1},{1,0},{2,3},{3,2},{4,5},{5,4},{6,7},{7,6},{8,9},{9,8},{10,11... | collective-permute-start | bytes 2359304 | tf_op jit(solution)/shard_map/ppermute | solution.py:103
  74.1 1.3 multiply_convert_fusion
  75.4 1.1 reshape.480
  76.5 0.0 collective-permute-done.3
  76.5 0.0 collective-permute-done.4
  76.5 0.0 collective-permute-done.5
  76.5 7.9 %all-to-all-start.1 = ((bf16[64,32,128]{2,1,0:T(8,128)(2,1)}), bf16[64,32,128]{2,1,0:T(8,128)(2,1)S(1)}, u32[]{:S(2)}, u32[]{:S(2)}) async-start(bf16[64,32,128]{2,1,0:T(8,128)(2,1)} %reshape.480), calls=%async_computation.1 | async-start | bytes 1048576 | tf_op jit(solution)/shard_map/all_to_all | solution.py:180
  84.4 0.0 collective-permute-done.8.refs_2_
  84.4 3.4 %collective-permute-start.12 = (bf16[64,48,128]{2,1,0:T(8,128)(2,1)}, bf16[64,48,128]{2,1,0:T(8,128)(2,1)}, u32[]{:S(2)}, u32[]{:S(2)}) collective-permute-start(bf16[64,48,128]{2,1,0:T(8,128)(2,1)} %collective-permute-done.8.refs_2_), channel_id=1, source_target_pairs={{0,2},{1,7},{2,4},{3,1},{4,6},{5,3},{6,0},{7,5},{8,10},{9,15},{10,... | collective-permute-start | bytes 2359304 | tf_op jit(solution)/shard_map/ppermute | solution.py:100
  87.8 0.0 collective-permute-done.7.refs_1_
  87.8 3.2 %collective-permute-start.10 = (bf16[64,48,128]{2,1,0:T(8,128)(2,1)}, bf16[64,48,128]{2,1,0:T(8,128)(2,1)}, u32[]{:S(2)}, u32[]{:S(2)}) collective-permute-start(bf16[64,48,128]{2,1,0:T(8,128)(2,1)} %collective-permute-done.7.refs_1_), channel_id=1, source_target_pairs={{0,2},{1,7},{2,4},{3,1},{4,6},{5,3},{6,0},{7,5},{8,10},{9,15},{10,... | collective-permute-start | bytes 2359304 | tf_op jit(solution)/shard_map/ppermute | solution.py:100
  91.0 2.2 %collective-permute-start.9 = (bf16[64,48,128]{2,1,0:T(8,128)(2,1)}, bf16[64,48,128]{2,1,0:T(8,128)(2,1)}, u32[]{:S(2)}, u32[]{:S(2)}) collective-permute-start(bf16[64,48,128]{2,1,0:T(8,128)(2,1)} %collective-permute-done.8.refs_2_), channel_id=1, source_target_pairs={{0,1},{1,0},{2,3},{3,2},{4,5},{5,4},{6,7},{7,6},{8,9},{9,8},{10,11... | collective-permute-start | bytes 2359304 | tf_op jit(solution)/shard_map/ppermute | solution.py:103
  93.2 4.6 %collective-permute-done.12.refs_6_ = bf16[64,48,128]{2,1,0:T(8,128)(2,1)} collective-permute-done((bf16[64,48,128]{2,1,0:T(8,128)(2,1)}, bf16[64,48,128]{2,1,0:T(8,128)(2,1)}, u32[]{:S(2)}, u32[]{:S(2)}) %collective-permute-start.12) | collective-permute-done | bytes 786464 | tf_op jit(solution)/shard_map/ppermute | solution.py:100
  97.8 4.3 %collective-permute-start.13 = (bf16[64,48,128]{2,1,0:T(8,128)(2,1)}, bf16[64,48,128]{2,1,0:T(8,128)(2,1)}, u32[]{:S(2)}, u32[]{:S(2)}) collective-permute-start(bf16[64,48,128]{2,1,0:T(8,128)(2,1)} %collective-permute-done.12.refs_6_), channel_id=1, source_target_pairs={{0,1},{1,0},{2,3},{3,2},{4,5},{5,4},{6,7},{7,6},{8,9},{9,8},{10,11... | collective-permute-start | bytes 2359304 | tf_op jit(solution)/shard_map/ppermute | solution.py:103
  102.0 4.2 %collective-permute-done.10.refs_4_ = bf16[64,48,128]{2,1,0:T(8,128)(2,1)} collective-permute-done((bf16[64,48,128]{2,1,0:T(8,128)(2,1)}, bf16[64,48,128]{2,1,0:T(8,128)(2,1)}, u32[]{:S(2)}, u32[]{:S(2)}) %collective-permute-start.10) | collective-permute-done | bytes 786464 | tf_op jit(solution)/shard_map/ppermute | solution.py:100
  106.2 4.3 %collective-permute-start.11 = (bf16[64,48,128]{2,1,0:T(8,128)(2,1)}, bf16[64,48,128]{2,1,0:T(8,128)(2,1)}, u32[]{:S(2)}, u32[]{:S(2)}) collective-permute-start(bf16[64,48,128]{2,1,0:T(8,128)(2,1)} %collective-permute-done.10.refs_4_), channel_id=1, source_target_pairs={{0,1},{1,0},{2,3},{3,2},{4,5},{5,4},{6,7},{7,6},{8,9},{9,8},{10,11... | collective-permute-start | bytes 2359304 | tf_op jit(solution)/shard_map/ppermute | solution.py:103
  110.5 5.3 %all-to-all-done.1 = bf16[64,32,128]{2,1,0:T(8,128)(2,1)S(1)} async-done(((bf16[64,32,128]{2,1,0:T(8,128)(2,1)}), bf16[64,32,128]{2,1,0:T(8,128)(2,1)S(1)}, u32[]{:S(2)}, u32[]{:S(2)}) %all-to-all-start.1) | async-done | bytes 524320 | tf_op jit(solution)/shard_map/all_to_all | solution.py:180
  115.8 1.0 reshape.481.x_ref
  116.8 0.0 collective-permute-done.9.refs_3_
  116.8 0.0 collective-permute-done.13.refs_7_
  116.8 0.0 collective-permute-done.11.refs_5_
  116.8 5.1 %expert.1 = bf16[64,16,256]{2,1,0:T(8,128)(2,1)} custom-call(bf16[128,2048]{1,0:T(8,128)(2,1)} %reshape.481.x_ref, bf16[64,48,128]{2,1,0:T(8,128)(2,1)} %copy-done.1, bf16[64,48,128]{2,1,0:T(8,128)(2,1)} %collective-permute-done.7.refs_1_, bf16[64,48,128]{2,1,0:T(8,128)(2,1)} %collective-permute-done.8.refs_2_, ...), custom_call_target="tpu_custom_call" | custom-call | tf_op jit(solution)/shard_map/expert/pallas_call | solution.py:85
  121.9 9.8 %all-to-all-start.2 = ((bf16[64,16,256]{2,1,0:T(8,128)(2,1)}), bf16[64,16,256]{2,1,0:T(8,128)(2,1)S(1)}, u32[]{:S(2)}, u32[]{:S(2)}) async-start(bf16[64,16,256]{2,1,0:T(8,128)(2,1)} %expert.1), calls=%async_computation.2 | async-start | bytes 1048576 | tf_op jit(solution)/shard_map/all_to_all | solution.py:195
  131.7 1.9 %collective-permute-start.6 = (bf16[8,64]{1,0:T(8,128)(2,1)S(1)}, bf16[8,64]{1,0:T(8,128)(2,1)S(1)}, u32[]{:S(2)}, u32[]{:S(2)}) collective-permute-start(bf16[8,64]{1,0:T(8,128)(2,1)S(1)} %bitcast.104), channel_id=1, source_target_pairs={{0,448},{64,0},{128,64},{192,128},{256,192},{320,256},{384,320},{4... | collective-permute-start | bytes 3080 | tf_op jit(solution)/shard_map/ppermute | solution.py:119
  133.8 3.5 %collective-permute-done.6 = bf16[8,64]{1,0:T(8,128)(2,1)S(1)} collective-permute-done((bf16[8,64]{1,0:T(8,128)(2,1)S(1)}, bf16[8,64]{1,0:T(8,128)(2,1)S(1)}, u32[]{:S(2)}, u32[]{:S(2)}) %collective-permute-start.6) | collective-permute-done | bytes 1056 | tf_op jit(solution)/shard_map/ppermute | solution.py:119
  137.3 0.1 stack.53
  137.3 0.2 convolution_bitcast_fusion
  137.5 0.1 convert_element_type.111
  137.6 0.1 broadcast_in_dim.50
  137.7 0.1 broadcast_in_dim.52
  137.8 6.1 %all-to-all-done.2 = bf16[64,16,256]{2,1,0:T(8,128)(2,1)S(1)} async-done(((bf16[64,16,256]{2,1,0:T(8,128)(2,1)}), bf16[64,16,256]{2,1,0:T(8,128)(2,1)S(1)}, u32[]{:S(2)}, u32[]{:S(2)}) %all-to-all-start.2) | async-done | bytes 524320 | tf_op jit(solution)/shard_map/all_to_all | solution.py:195
  143.9 1.3 convolution_convert_fusion
  145.3 4.1 %all-to-all-start.3 = ((bf16[8,64,256]{2,1,0:T(8,128)(2,1)}), bf16[8,64,256]{2,1,0:T(8,128)(2,1)}, u32[]{:S(2)}, u32[]{:S(2)}) async-start(bf16[8,64,256]{2,1,0:T(8,128)(2,1)} %bitcast.80), calls=%async_computation.3 | async-start | bytes 524288 | tf_op jit(solution)/shard_map/all_to_all | solution.py:199
  149.3 0.6 multiply_add_fusion.1.slot_ref
  149.9 0.1 fusion.50
  150.1 0.1 pad_maximum_fusion
  150.2 0.9 copy.31
  151.1 1.0 fusion.51
  152.1 1.9 %copy.29 = bf16[1,2048,64]{1,2,0:T(8,128)(2,1)} copy(bf16[1,2048,64]{2,1,0:T(8,128)(2,1)} %bitcast.78) | data formatting | bytes 524288
  154.0 0.9 copy.30
  154.9 15.8 %all-to-all-done.3 = bf16[8,64,256]{2,1,0:T(8,128)(2,1)} async-done(((bf16[8,64,256]{2,1,0:T(8,128)(2,1)}), bf16[8,64,256]{2,1,0:T(8,128)(2,1)}, u32[]{:S(2)}, u32[]{:S(2)}) %all-to-all-start.3) | async-done | bytes 262176 | tf_op jit(solution)/shard_map/all_to_all | solution.py:199
  170.7 2.2 %home.1 = bf16[512,256]{1,0:T(8,128)(2,1)} custom-call(s32[1,512]{1,0:T(1,128)} %multiply_add_fusion.1.slot_ref, bf16[512,256]{1,0:T(8,128)(2,1)} %bitcast.37.back_ref), custom_call_target="tpu_custom_call" | custom-call | tf_op jit(solution)/shard_map/home/pallas_call | solution.py:202
  (44 shorter events, 0.4 us)
Async XLA Ops:
  0.6 52.6 %copy-start = (bf16[512,2048]{1,0:T(8,128)(2,1)S(1)}, bf16[512,2048]{1,0:T(8,128)(2,1)}, u32[]{:S(2)}) copy-start(bf16[512,2048]{1,0:T(8,128)(2,1)} %param.8) | copy-start | bytes 6291460
  0.6 22.9 %copy-start.3 = (s32[512,2]{0,1:T(2,128)S(1)}, s32[512,2]{0,1:T(2,128)}, u32[]{:S(2)}) copy-start(s32[512,2]{0,1:T(2,128)} %param.13) | copy-start | bytes 12292
  4.1 19.8 %copy-start.4 = (f32[512,2]{0,1:T(2,128)S(1)}, f32[512,2]{0,1:T(2,128)}, u32[]{:S(2)}) copy-start(f32[512,2]{0,1:T(2,128)} %param.15) | copy-start | bytes 12292
  4.1 19.8 %copy-start.5 = (f32[512]{0:T(512)S(1)}, f32[512]{0:T(512)}, u32[]{:S(2)}) copy-start(f32[512]{0:T(512)} %param.14) | copy-start | bytes 6148
  4.1 60.3 %all-to-all-start = ((bf16[64,48,128]{2,1,0:T(8,128)(2,1)}), bf16[64,48,128]{2,1,0:T(8,128)(2,1)S(1)}, u32[]{:S(2)}, u32[]{:S(2)}) async-start(bf16[64,48,128]{2,1,0:T(8,128)(2,1)} %pack.1), calls=%async_computation | async-start | bytes 1572864 | tf_op jit(solution)/shard_map/all_to_all | solution.py:126
  24.6 31.5 %collective-permute-start = (bf16[8,64]{1,0:T(8,128)(2,1)S(1)}, bf16[8,64]{1,0:T(8,128)(2,1)S(1)}, u32[]{:S(2)}, u32[]{:S(2)}) collective-permute-start(bf16[8,64]{1,0:T(8,128)(2,1)S(1)} %bitcast.102), channel_id=1, source_target_pairs={{0,64},{64,128},{128,192},{192,256},{256,320},{320,384},{384,448},... | collective-permute-start | bytes 3080 | tf_op jit(solution)/shard_map/ppermute | solution.py:119
  28.5 34.3 %collective-permute-start.1 = (bf16[8,64]{1,0:T(8,128)(2,1)S(1)}, bf16[8,64]{1,0:T(8,128)(2,1)S(1)}, u32[]{:S(2)}, u32[]{:S(2)}) collective-permute-start(bf16[8,64]{1,0:T(8,128)(2,1)S(1)} %bitcast.101), channel_id=1, source_target_pairs={{0,128},{64,192},{128,256},{192,320},{256,384},{320,448},{384,0},{... | collective-permute-start | bytes 3080 | tf_op jit(solution)/shard_map/ppermute | solution.py:119
  35.5 33.3 %collective-permute-start.2 = (bf16[8,64]{1,0:T(8,128)(2,1)S(1)}, bf16[8,64]{1,0:T(8,128)(2,1)S(1)}, u32[]{:S(2)}, u32[]{:S(2)}) collective-permute-start(bf16[8,64]{1,0:T(8,128)(2,1)S(1)} %bitcast.100), channel_id=1, source_target_pairs={{0,192},{64,256},{128,320},{192,384},{256,448},{320,0},{384,64},{4... | collective-permute-start | bytes 3080 | tf_op jit(solution)/shard_map/ppermute | solution.py:119
  40.9 35.6 %collective-permute-start.3 = (bf16[8,64]{1,0:T(8,128)(2,1)S(1)}, bf16[8,64]{1,0:T(8,128)(2,1)S(1)}, u32[]{:S(2)}, u32[]{:S(2)}) collective-permute-start(bf16[8,64]{1,0:T(8,128)(2,1)S(1)} %bitcast.98), channel_id=1, source_target_pairs={{0,256},{64,320},{128,384},{192,448},{256,0},{320,64},{384,128},{4... | collective-permute-start | bytes 3080 | tf_op jit(solution)/shard_map/ppermute | solution.py:119
  47.7 28.8 %collective-permute-start.4 = (bf16[8,64]{1,0:T(8,128)(2,1)S(1)}, bf16[8,64]{1,0:T(8,128)(2,1)S(1)}, u32[]{:S(2)}, u32[]{:S(2)}) collective-permute-start(bf16[8,64]{1,0:T(8,128)(2,1)S(1)} %bitcast.99), channel_id=1, source_target_pairs={{0,320},{64,384},{128,448},{192,0},{256,64},{320,128},{384,192},{4... | collective-permute-start | bytes 3080 | tf_op jit(solution)/shard_map/ppermute | solution.py:119
  56.1 20.4 %collective-permute-start.5 = (bf16[8,64]{1,0:T(8,128)(2,1)S(1)}, bf16[8,64]{1,0:T(8,128)(2,1)S(1)}, u32[]{:S(2)}, u32[]{:S(2)}) collective-permute-start(bf16[8,64]{1,0:T(8,128)(2,1)S(1)} %bitcast.103), channel_id=1, source_target_pairs={{0,384},{64,448},{128,0},{192,64},{256,128},{320,192},{384,256},{4... | collective-permute-start | bytes 3080 | tf_op jit(solution)/shard_map/ppermute | solution.py:119
  64.4 52.4 %copy-start.1 = (bf16[64,48,128]{2,1,0:T(8,128)(2,1)}, bf16[64,48,128]{2,1,0:T(8,128)(2,1)S(1)}, u32[]{:S(2)}) copy-start(bf16[64,48,128]{2,1,0:T(8,128)(2,1)S(1)} %all-to-all-done.refs_0_) | copy-start | bytes 2359300
  64.4 20.0 %collective-permute-start.8 = (bf16[64,48,128]{2,1,0:T(8,128)(2,1)S(1)}, bf16[64,48,128]{2,1,0:T(8,128)(2,1)}, u32[]{:S(2)}, u32[]{:S(2)}) collective-permute-start(bf16[64,48,128]{2,1,0:T(8,128)(2,1)S(1)} %all-to-all-done.refs_0_), channel_id=1, source_target_pairs={{0,2},{1,7},{2,4},{3,1},{4,6},{5,3},{6,0},{7,5},{8,10},{9,15},{10,... | collective-permute-start | bytes 2359304 | tf_op jit(solution)/shard_map/ppermute | solution.py:100
  68.8 19.0 %collective-permute-start.7 = (bf16[64,48,128]{2,1,0:T(8,128)(2,1)S(1)}, bf16[64,48,128]{2,1,0:T(8,128)(2,1)}, u32[]{:S(2)}, u32[]{:S(2)}) collective-permute-start(bf16[64,48,128]{2,1,0:T(8,128)(2,1)S(1)} %all-to-all-done.refs_0_), channel_id=1, source_target_pairs={{0,1},{1,0},{2,3},{3,2},{4,5},{5,4},{6,7},{7,6},{8,9},{9,8},{10,11... | collective-permute-start | bytes 2359304 | tf_op jit(solution)/shard_map/ppermute | solution.py:103
  76.5 39.3 %all-to-all-start.1 = ((bf16[64,32,128]{2,1,0:T(8,128)(2,1)}), bf16[64,32,128]{2,1,0:T(8,128)(2,1)S(1)}, u32[]{:S(2)}, u32[]{:S(2)}) async-start(bf16[64,32,128]{2,1,0:T(8,128)(2,1)} %reshape.480), calls=%async_computation.1 | async-start | bytes 1048576 | tf_op jit(solution)/shard_map/all_to_all | solution.py:180
  84.4 13.3 %collective-permute-start.12 = (bf16[64,48,128]{2,1,0:T(8,128)(2,1)}, bf16[64,48,128]{2,1,0:T(8,128)(2,1)}, u32[]{:S(2)}, u32[]{:S(2)}) collective-permute-start(bf16[64,48,128]{2,1,0:T(8,128)(2,1)} %collective-permute-done.8.refs_2_), channel_id=1, source_target_pairs={{0,2},{1,7},{2,4},{3,1},{4,6},{5,3},{6,0},{7,5},{8,10},{9,15},{10,... | collective-permute-start | bytes 2359304 | tf_op jit(solution)/shard_map/ppermute | solution.py:100
  87.8 18.4 %collective-permute-start.10 = (bf16[64,48,128]{2,1,0:T(8,128)(2,1)}, bf16[64,48,128]{2,1,0:T(8,128)(2,1)}, u32[]{:S(2)}, u32[]{:S(2)}) collective-permute-start(bf16[64,48,128]{2,1,0:T(8,128)(2,1)} %collective-permute-done.7.refs_1_), channel_id=1, source_target_pairs={{0,2},{1,7},{2,4},{3,1},{4,6},{5,3},{6,0},{7,5},{8,10},{9,15},{10,... | collective-permute-start | bytes 2359304 | tf_op jit(solution)/shard_map/ppermute | solution.py:100
  91.0 25.8 %collective-permute-start.9 = (bf16[64,48,128]{2,1,0:T(8,128)(2,1)}, bf16[64,48,128]{2,1,0:T(8,128)(2,1)}, u32[]{:S(2)}, u32[]{:S(2)}) collective-permute-start(bf16[64,48,128]{2,1,0:T(8,128)(2,1)} %collective-permute-done.8.refs_2_), channel_id=1, source_target_pairs={{0,1},{1,0},{2,3},{3,2},{4,5},{5,4},{6,7},{7,6},{8,9},{9,8},{10,11... | collective-permute-start | bytes 2359304 | tf_op jit(solution)/shard_map/ppermute | solution.py:103
  97.8 19.1 %collective-permute-start.13 = (bf16[64,48,128]{2,1,0:T(8,128)(2,1)}, bf16[64,48,128]{2,1,0:T(8,128)(2,1)}, u32[]{:S(2)}, u32[]{:S(2)}) collective-permute-start(bf16[64,48,128]{2,1,0:T(8,128)(2,1)} %collective-permute-done.12.refs_6_), channel_id=1, source_target_pairs={{0,1},{1,0},{2,3},{3,2},{4,5},{5,4},{6,7},{7,6},{8,9},{9,8},{10,11... | collective-permute-start | bytes 2359304 | tf_op jit(solution)/shard_map/ppermute | solution.py:103
  106.2 10.7 %collective-permute-start.11 = (bf16[64,48,128]{2,1,0:T(8,128)(2,1)}, bf16[64,48,128]{2,1,0:T(8,128)(2,1)}, u32[]{:S(2)}, u32[]{:S(2)}) collective-permute-start(bf16[64,48,128]{2,1,0:T(8,128)(2,1)} %collective-permute-done.10.refs_4_), channel_id=1, source_target_pairs={{0,1},{1,0},{2,3},{3,2},{4,5},{5,4},{6,7},{7,6},{8,9},{9,8},{10,11... | collective-permute-start | bytes 2359304 | tf_op jit(solution)/shard_map/ppermute | solution.py:103
  121.9 22.0 %all-to-all-start.2 = ((bf16[64,16,256]{2,1,0:T(8,128)(2,1)}), bf16[64,16,256]{2,1,0:T(8,128)(2,1)S(1)}, u32[]{:S(2)}, u32[]{:S(2)}) async-start(bf16[64,16,256]{2,1,0:T(8,128)(2,1)} %expert.1), calls=%async_computation.2 | async-start | bytes 1048576 | tf_op jit(solution)/shard_map/all_to_all | solution.py:195
  131.7 5.5 %collective-permute-start.6 = (bf16[8,64]{1,0:T(8,128)(2,1)S(1)}, bf16[8,64]{1,0:T(8,128)(2,1)S(1)}, u32[]{:S(2)}, u32[]{:S(2)}) collective-permute-start(bf16[8,64]{1,0:T(8,128)(2,1)S(1)} %bitcast.104), channel_id=1, source_target_pairs={{0,448},{64,0},{128,64},{192,128},{256,192},{320,256},{384,320},{4... | collective-permute-start | bytes 3080 | tf_op jit(solution)/shard_map/ppermute | solution.py:119
  143.9 6.0 %copy-start.2 = (bf16[64,48,128]{2,1,0:T(8,128)(2,1)S(1)}, bf16[64,48,128]{2,1,0:T(8,128)(2,1)}, u32[]{:S(2)}) copy-start(bf16[64,48,128]{2,1,0:T(8,128)(2,1)} %copy-done.1) | copy-start | bytes 2359300
  145.3 25.4 %all-to-all-start.3 = ((bf16[8,64,256]{2,1,0:T(8,128)(2,1)}), bf16[8,64,256]{2,1,0:T(8,128)(2,1)}, u32[]{:S(2)}, u32[]{:S(2)}) async-start(bf16[8,64,256]{2,1,0:T(8,128)(2,1)} %bitcast.80), calls=%async_computation.3 | async-start | bytes 524288 | tf_op jit(solution)/shard_map/all_to_all | solution.py:199

commit v4 on v3

--- a/solution.py
+++ b/solution.py
@@ -12,6 +12,9 @@
 IN_GROUP = ("l", "y", "x", "c")
 BF = jnp.bfloat16
 F32 = jnp.float32
+
+
+HELD = (0, 6, 8)
 
 
 def pack_kernel(gain_ref, gate_ref, up_ref, down_ref, out_ref):
@@ -82,12 +85,15 @@
 
 
 def expert(rows, shards):
+    operands = [rows, *shards]
+    for i in HELD:
+        operands[i] = pltpu.with_memory_space_constraint(operands[i], pltpu.VMEM)
     return pl.pallas_call(
         expert_kernel,
         out_shape=jax.ShapeDtypeStruct((64, 16, 256), BF),
         scratch_shapes=[pltpu.VMEM((256, 1024), F32)],
         name="expert",
-    )(rows, *shards)
+    )(*operands)
 
 
 def gather_weights(own):
@@ -201,7 +207,7 @@
     ).reshape(512, 256)
     home = pl.pallas_call(
         home_kernel, out_shape=jax.ShapeDtypeStruct((512, 256), BF), name="home"
-    )(slot.reshape(1, 512), home)
+    )(slot.reshape(1, 512), pltpu.with_memory_space_constraint(home, pltpu.VMEM))
     return new_gate, new_up, new_down, home
 
 

time: 174 us -> 170 us (0.977)
  starting transfers between devices: 105 us -> 108 us
  local copies, waits for them, and re-layouts: 7.56 us -> 4.91 us
  waiting for transfers between devices: 42.6 us -> 40.5 us
    unnamed x22 -> x20, local copies, waits for them, and re-layouts: 3.79 us -> 2.75 us
  transfers between devices with their start and end apart: 18 -> 18, of which waited for: 8 -> 8; matrix products, arithmetic and copies ran while one was open for 7% -> 5% of each run, Pallas kernels for 0% -> 0%
where the time goes in v4:
time: 170 us
  starting transfers between devices  108 us (64%)
  waiting for transfers between devices  40.5 us (24%)
  Pallas kernels  9.67 us (6%)
  local copies, waits for them, and re-layouts  4.91 us (3%)
  matrix products  4.28 us (3%)
    ppermute x7, starting transfers between devices, trade_facts(): part = lax.ppermute(part, 'g', [(i, (i + k) % 8) for i in range(8)])  37.1 us
    all_to_all x1, starting transfers between devices, local(): own = lax.all_to_all(packed, FS, split_axis=0, concat_axis=0, tiled=True)  19.4 us
    ppermute x4, starting transfers between devices, swap(): return lax.ppermute(v, 'c', [(0, 1), (1, 0)])  17.5 us
    all_to_all x1, waiting for transfers between devices, local(): lax.all_to_all(mixed.reshape(8, 64, 256), 'g', split_axis=0, concat_axis=...  16.4 us
    ppermute x3, starting transfers between devices, pass_on(): return lax.ppermute(v, TP, around)  10.9 us
    all_to_all x1, starting transfers between devices, local(): lax.all_to_all(outs, IN_GROUP, split_axis=0, concat_axis=0, tiled=True)  10.2 us
    all_to_all x1, starting transfers between devices, local(): lax.all_to_all(sent, ('l', 'y', 'g'), split_axis=0, concat_axis=0, tiled=...  7.9 us
    ppermute x3, waiting for transfers between devices, pass_on(): return lax.ppermute(v, TP, around)  7.68 us
  transfers between devices with their start and end apart: 18, of which 8 were waited for; matrix products, arithmetic and copies ran while one was open for 5% of the time, Pallas kernels for 0%

profile of v4, /device:TPU:1, one launch (start us, length us, event | category | flops | bytes accessed | tf_op | source)
XLA Modules:
  0.0 169.5 jit_solution(5694687852366685203)
XLA Ops:
  0.6 0.0 copy-start.2
  0.6 3.3 %pack.1 = bf16[64,48,128]{2,1,0:T(8,128)(2,1)} custom-call(f32[1,32]{1,0:T(1,128)} %bitcast.109, f32[64,32,64]{2,1,0:T(8,128)} %gate_ref.1, f32[64,32,64]{2,1,0:T(8,128)} %up_ref.1, f32[64,32,64]{2,1,0:T(8,128)} %down_ref.1), custom_call_target="tpu_custom_call" | custom-call | tf_op jit(solution)/shard_map/pack/pallas_call | solution.py:33
  4.0 19.4 %all-to-all-start = ((bf16[64,48,128]{2,1,0:T(8,128)(2,1)}), bf16[64,48,128]{2,1,0:T(8,128)(2,1)S(1)}, u32[]{:S(2)}, u32[]{:S(2)}) async-start(bf16[64,48,128]{2,1,0:T(8,128)(2,1)} %pack.1), calls=%async_computation | async-start | bytes 1572864 | tf_op jit(solution)/shard_map/all_to_all | solution.py:132
  23.4 0.0 copy-done.2
  23.4 0.3 select_reduce_fusion.1
  23.8 0.0 copy-done.3
  23.8 0.0 copy-done.4
  24.0 0.3 convolution_convert_fusion.1
  24.3 0.1 reshape.479
  24.4 3.8 %collective-permute-start = (bf16[8,64]{1,0:T(8,128)(2,1)S(1)}, bf16[8,64]{1,0:T(8,128)(2,1)S(1)}, u32[]{:S(2)}, u32[]{:S(2)}) collective-permute-start(bf16[8,64]{1,0:T(8,128)(2,1)S(1)} %bitcast.102), channel_id=1, source_target_pairs={{0,64},{64,128},{128,192},{192,256},{256,320},{320,384},{384,448},... | collective-permute-start | bytes 3080 | tf_op jit(solution)/shard_map/ppermute | solution.py:125
  28.3 7.0 %collective-permute-start.1 = (bf16[8,64]{1,0:T(8,128)(2,1)S(1)}, bf16[8,64]{1,0:T(8,128)(2,1)S(1)}, u32[]{:S(2)}, u32[]{:S(2)}) collective-permute-start(bf16[8,64]{1,0:T(8,128)(2,1)S(1)} %bitcast.101), channel_id=1, source_target_pairs={{0,128},{64,192},{128,256},{192,320},{256,384},{320,448},{384,0},{... | collective-permute-start | bytes 3080 | tf_op jit(solution)/shard_map/ppermute | solution.py:125
  35.3 5.4 %collective-permute-start.2 = (bf16[8,64]{1,0:T(8,128)(2,1)S(1)}, bf16[8,64]{1,0:T(8,128)(2,1)S(1)}, u32[]{:S(2)}, u32[]{:S(2)}) collective-permute-start(bf16[8,64]{1,0:T(8,128)(2,1)S(1)} %bitcast.100), channel_id=1, source_target_pairs={{0,192},{64,256},{128,320},{192,384},{256,448},{320,0},{384,64},{4... | collective-permute-start | bytes 3080 | tf_op jit(solution)/shard_map/ppermute | solution.py:125
  40.7 6.8 %collective-permute-start.3 = (bf16[8,64]{1,0:T(8,128)(2,1)S(1)}, bf16[8,64]{1,0:T(8,128)(2,1)S(1)}, u32[]{:S(2)}, u32[]{:S(2)}) collective-permute-start(bf16[8,64]{1,0:T(8,128)(2,1)S(1)} %bitcast.98), channel_id=1, source_target_pairs={{0,256},{64,320},{128,384},{192,448},{256,0},{320,64},{384,128},{4... | collective-permute-start | bytes 3080 | tf_op jit(solution)/shard_map/ppermute | solution.py:125
  47.5 5.5 %collective-permute-start.4 = (bf16[8,64]{1,0:T(8,128)(2,1)S(1)}, bf16[8,64]{1,0:T(8,128)(2,1)S(1)}, u32[]{:S(2)}, u32[]{:S(2)}) collective-permute-start(bf16[8,64]{1,0:T(8,128)(2,1)S(1)} %bitcast.99), channel_id=1, source_target_pairs={{0,320},{64,384},{128,448},{192,0},{256,64},{320,128},{384,192},{4... | collective-permute-start | bytes 3080 | tf_op jit(solution)/shard_map/ppermute | solution.py:125
  53.0 2.1 %multiply_reduce_fusion = (f32[128]{0:T(128)S(1)}, f32[128,2048]{1,0:T(8,128)S(1)}) fusion(bf16[512,2048]{1,0:T(8,128)(2,1)} %param.8, s32[512]{0:T(512)S(1)} %get-tuple-element.58, s32[512]{0:T(512)S(1)} %get-tuple-element.57), kind=kOutput, calls=%fused_computation.12 | convolution fusion | flops 269156224 | bytes 3150336 | tf_op jit(solution)/shard_map/dot_general | solution.py:161
  55.2 0.8 collective-permute-done
  56.0 6.6 %collective-permute-start.5 = (bf16[8,64]{1,0:T(8,128)(2,1)S(1)}, bf16[8,64]{1,0:T(8,128)(2,1)S(1)}, u32[]{:S(2)}, u32[]{:S(2)}) collective-permute-start(bf16[8,64]{1,0:T(8,128)(2,1)S(1)} %bitcast.103), channel_id=1, source_target_pairs={{0,384},{64,448},{128,0},{192,64},{256,128},{320,192},{384,256},{4... | collective-permute-start | bytes 3080 | tf_op jit(solution)/shard_map/ppermute | solution.py:125
  62.6 0.0 collective-permute-done.1
  62.6 1.6 all-to-all-done.refs_0_
  64.2 4.4 %collective-permute-start.8 = (bf16[64,48,128]{2,1,0:T(8,128)(2,1)S(1)}, bf16[64,48,128]{2,1,0:T(8,128)(2,1)}, u32[]{:S(2)}, u32[]{:S(2)}) collective-permute-start(bf16[64,48,128]{2,1,0:T(8,128)(2,1)S(1)} %all-to-all-done.refs_0_), channel_id=1, source_target_pairs={{0,2},{1,7},{2,4},{3,1},{4,6},{5,3},{6,0},{7,5},{8,10},{9,15},{10,... | collective-permute-start | bytes 2359304 | tf_op jit(solution)/shard_map/ppermute | solution.py:106
  68.6 0.0 collective-permute-done.2
  68.6 5.3 %collective-permute-start.7 = (bf16[64,48,128]{2,1,0:T(8,128)(2,1)S(1)}, bf16[64,48,128]{2,1,0:T(8,128)(2,1)}, u32[]{:S(2)}, u32[]{:S(2)}) collective-permute-start(bf16[64,48,128]{2,1,0:T(8,128)(2,1)S(1)} %all-to-all-done.refs_0_), channel_id=1, source_target_pairs={{0,1},{1,0},{2,3},{3,2},{4,5},{5,4},{6,7},{7,6},{8,9},{9,8},{10,11... | collective-permute-start | bytes 2359304 | tf_op jit(solution)/shard_map/ppermute | solution.py:109
  73.9 0.1 multiply_convert_fusion
  74.0 1.0 reshape.480
  75.1 0.0 collective-permute-done.3
  75.1 0.0 collective-permute-done.4
  75.1 0.0 collective-permute-done.5
  75.1 7.9 %all-to-all-start.1 = ((bf16[64,32,128]{2,1,0:T(8,128)(2,1)}), bf16[64,32,128]{2,1,0:T(8,128)(2,1)S(1)}, u32[]{:S(2)}, u32[]{:S(2)}) async-start(bf16[64,32,128]{2,1,0:T(8,128)(2,1)} %reshape.480), calls=%async_computation.1 | async-start | bytes 1048576 | tf_op jit(solution)/shard_map/all_to_all | solution.py:186
  83.0 0.0 collective-permute-done.8.refs_2_
  83.0 3.4 %collective-permute-start.12 = (bf16[64,48,128]{2,1,0:T(8,128)(2,1)}, bf16[64,48,128]{2,1,0:T(8,128)(2,1)}, u32[]{:S(2)}, u32[]{:S(2)}) collective-permute-start(bf16[64,48,128]{2,1,0:T(8,128)(2,1)} %collective-permute-done.8.refs_2_), channel_id=1, source_target_pairs={{0,2},{1,7},{2,4},{3,1},{4,6},{5,3},{6,0},{7,5},{8,10},{9,15},{10,... | collective-permute-start | bytes 2359304 | tf_op jit(solution)/shard_map/ppermute | solution.py:106
  86.4 0.0 collective-permute-done.7.refs_1_
  86.4 3.2 %collective-permute-start.10 = (bf16[64,48,128]{2,1,0:T(8,128)(2,1)}, bf16[64,48,128]{2,1,0:T(8,128)(2,1)}, u32[]{:S(2)}, u32[]{:S(2)}) collective-permute-start(bf16[64,48,128]{2,1,0:T(8,128)(2,1)} %collective-permute-done.7.refs_1_), channel_id=1, source_target_pairs={{0,2},{1,7},{2,4},{3,1},{4,6},{5,3},{6,0},{7,5},{8,10},{9,15},{10,... | collective-permute-start | bytes 2359304 | tf_op jit(solution)/shard_map/ppermute | solution.py:106
  89.6 2.8 %collective-permute-start.9 = (bf16[64,48,128]{2,1,0:T(8,128)(2,1)}, bf16[64,48,128]{2,1,0:T(8,128)(2,1)}, u32[]{:S(2)}, u32[]{:S(2)}) collective-permute-start(bf16[64,48,128]{2,1,0:T(8,128)(2,1)} %collective-permute-done.8.refs_2_), channel_id=1, source_target_pairs={{0,1},{1,0},{2,3},{3,2},{4,5},{5,4},{6,7},{7,6},{8,9},{9,8},{10,11... | collective-permute-start | bytes 2359304 | tf_op jit(solution)/shard_map/ppermute | solution.py:109
  92.4 4.0 %collective-permute-done.12.refs_6_ = bf16[64,48,128]{2,1,0:T(8,128)(2,1)} collective-permute-done((bf16[64,48,128]{2,1,0:T(8,128)(2,1)}, bf16[64,48,128]{2,1,0:T(8,128)(2,1)}, u32[]{:S(2)}, u32[]{:S(2)}) %collective-permute-start.12) | collective-permute-done | bytes 786464 | tf_op jit(solution)/shard_map/ppermute | solution.py:106
  96.3 4.7 %collective-permute-start.13 = (bf16[64,48,128]{2,1,0:T(8,128)(2,1)}, bf16[64,48,128]{2,1,0:T(8,128)(2,1)S(1)}, u32[]{:S(2)}, u32[]{:S(2)}) collective-permute-start(bf16[64,48,128]{2,1,0:T(8,128)(2,1)} %collective-permute-done.12.refs_6_), channel_id=1, source_target_pairs={{0,1},{1,0},{2,3},{3,2},{4,5},{5,4},{6,7},{7,6},{8,9},{9,8},{10,11... | collective-permute-start | bytes 2359304 | tf_op jit(solution)/shard_map/ppermute | solution.py:109
  101.1 3.7 %collective-permute-done.10.refs_4_ = bf16[64,48,128]{2,1,0:T(8,128)(2,1)} collective-permute-done((bf16[64,48,128]{2,1,0:T(8,128)(2,1)}, bf16[64,48,128]{2,1,0:T(8,128)(2,1)}, u32[]{:S(2)}, u32[]{:S(2)}) %collective-permute-start.10) | collective-permute-done | bytes 786464 | tf_op jit(solution)/shard_map/ppermute | solution.py:106
  104.8 4.7 %collective-permute-start.11 = (bf16[64,48,128]{2,1,0:T(8,128)(2,1)}, bf16[64,48,128]{2,1,0:T(8,128)(2,1)S(1)}, u32[]{:S(2)}, u32[]{:S(2)}) collective-permute-start(bf16[64,48,128]{2,1,0:T(8,128)(2,1)} %collective-permute-done.10.refs_4_), channel_id=1, source_target_pairs={{0,1},{1,0},{2,3},{3,2},{4,5},{5,4},{6,7},{7,6},{8,9},{9,8},{10,11... | collective-permute-start | bytes 2359304 | tf_op jit(solution)/shard_map/ppermute | solution.py:109
  109.5 4.5 %all-to-all-done.1 = bf16[64,32,128]{2,1,0:T(8,128)(2,1)S(1)} async-done(((bf16[64,32,128]{2,1,0:T(8,128)(2,1)}), bf16[64,32,128]{2,1,0:T(8,128)(2,1)S(1)}, u32[]{:S(2)}, u32[]{:S(2)}) %all-to-all-start.1) | async-done | bytes 524320 | tf_op jit(solution)/shard_map/all_to_all | solution.py:186
  114.0 0.2 reshape.481.x_ref
  114.2 0.0 copy-done
  114.2 0.0 collective-permute-done.9.refs_3_
  114.3 0.0 collective-permute-done.13.refs_7_
  114.3 0.0 collective-permute-done.11.refs_5_
  114.3 4.5 %expert.1 = bf16[64,16,256]{2,1,0:T(8,128)(2,1)} custom-call(bf16[128,2048]{1,0:T(8,128)(2,1)S(1)} %reshape.481.x_ref, bf16[64,48,128]{2,1,0:T(8,128)(2,1)} %copy-done, bf16[64,48,128]{2,1,0:T(8,128)(2,1)} %collective-permute-done.7.refs_1_, bf16[64,48,128]{2,1,0:T(8,128)(2,1)} %collective-permute-done.8.refs_2_, ...), custom_call_target="tpu_custom_call" | custom-call | tf_op jit(solution)/shard_map/expert/pallas_call | solution.py:91
  118.7 10.2 %all-to-all-start.2 = ((bf16[64,16,256]{2,1,0:T(8,128)(2,1)}), bf16[64,16,256]{2,1,0:T(8,128)(2,1)S(1)}, u32[]{:S(2)}, u32[]{:S(2)}) async-start(bf16[64,16,256]{2,1,0:T(8,128)(2,1)} %expert.1), calls=%async_computation.2 | async-start | bytes 1048576 | tf_op jit(solution)/shard_map/all_to_all | solution.py:201
  128.9 2.0 %collective-permute-start.6 = (bf16[8,64]{1,0:T(8,128)(2,1)S(1)}, bf16[8,64]{1,0:T(8,128)(2,1)S(1)}, u32[]{:S(2)}, u32[]{:S(2)}) collective-permute-start(bf16[8,64]{1,0:T(8,128)(2,1)S(1)} %bitcast.104), channel_id=1, source_target_pairs={{0,448},{64,0},{128,64},{192,128},{256,192},{320,256},{384,320},{4... | collective-permute-start | bytes 3080 | tf_op jit(solution)/shard_map/ppermute | solution.py:125
  131.0 3.4 %collective-permute-done.6 = bf16[8,64]{1,0:T(8,128)(2,1)S(1)} collective-permute-done((bf16[8,64]{1,0:T(8,128)(2,1)S(1)}, bf16[8,64]{1,0:T(8,128)(2,1)S(1)}, u32[]{:S(2)}, u32[]{:S(2)}) %collective-permute-start.6) | collective-permute-done | bytes 1056 | tf_op jit(solution)/shard_map/ppermute | solution.py:125
  134.4 0.1 stack.53
  134.5 0.2 convolution_bitcast_fusion
  134.7 0.1 convert_element_type.111
  134.8 0.1 broadcast_in_dim.50
  134.9 0.1 broadcast_in_dim.52
  135.0 6.1 %all-to-all-done.2 = bf16[64,16,256]{2,1,0:T(8,128)(2,1)S(1)} async-done(((bf16[64,16,256]{2,1,0:T(8,128)(2,1)}), bf16[64,16,256]{2,1,0:T(8,128)(2,1)S(1)}, u32[]{:S(2)}, u32[]{:S(2)}) %all-to-all-start.2) | async-done | bytes 524320 | tf_op jit(solution)/shard_map/all_to_all | solution.py:201
  141.1 1.3 convolution_convert_fusion
  142.5 5.0 %all-to-all-start.3 = ((bf16[8,64,256]{2,1,0:T(8,128)(2,1)}), bf16[8,64,256]{2,1,0:T(8,128)(2,1)S(1)}, u32[]{:S(2)}, u32[]{:S(2)}) async-start(bf16[8,64,256]{2,1,0:T(8,128)(2,1)} %bitcast.36), calls=%async_computation.3 | async-start | bytes 524288 | tf_op jit(solution)/shard_map/all_to_all | solution.py:205
  147.4 0.6 multiply_add_fusion.1.slot_ref
  148.0 0.1 fusion.50
  148.2 0.1 pad_maximum_fusion
  148.3 0.9 copy.31
  149.2 0.2 fusion.51
  149.4 0.9 copy.29
  150.3 0.9 copy.30
  151.2 16.4 %all-to-all-done.3 = bf16[8,64,256]{2,1,0:T(8,128)(2,1)S(1)} async-done(((bf16[8,64,256]{2,1,0:T(8,128)(2,1)}), bf16[8,64,256]{2,1,0:T(8,128)(2,1)S(1)}, u32[]{:S(2)}, u32[]{:S(2)}) %all-to-all-start.3) | async-done | bytes 262176 | tf_op jit(solution)/shard_map/all_to_all | solution.py:205
  167.6 1.9 %home.1 = bf16[512,256]{1,0:T(8,128)(2,1)} custom-call(s32[1,512]{1,0:T(1,128)} %multiply_add_fusion.1.slot_ref, bf16[512,256]{1,0:T(8,128)(2,1)S(1)} %bitcast.76), custom_call_target="tpu_custom_call" | custom-call | tf_op jit(solution)/shard_map/home/pallas_call | solution.py:208
  (42 shorter events, 0.4 us)
Async XLA Ops:
  0.6 22.8 %copy-start.2 = (s32[512,2]{0,1:T(2,128)S(1)}, s32[512,2]{0,1:T(2,128)}, u32[]{:S(2)}) copy-start(s32[512,2]{0,1:T(2,128)} %param.13) | copy-start | bytes 12292
  4.0 19.8 %copy-start.3 = (f32[512,2]{0,1:T(2,128)S(1)}, f32[512,2]{0,1:T(2,128)}, u32[]{:S(2)}) copy-start(f32[512,2]{0,1:T(2,128)} %param.15) | copy-start | bytes 12292
  4.0 19.8 %copy-start.4 = (f32[512]{0:T(512)S(1)}, f32[512]{0:T(512)}, u32[]{:S(2)}) copy-start(f32[512]{0:T(512)} %param.14) | copy-start | bytes 6148
  4.0 60.3 %all-to-all-start = ((bf16[64,48,128]{2,1,0:T(8,128)(2,1)}), bf16[64,48,128]{2,1,0:T(8,128)(2,1)S(1)}, u32[]{:S(2)}, u32[]{:S(2)}) async-start(bf16[64,48,128]{2,1,0:T(8,128)(2,1)} %pack.1), calls=%async_computation | async-start | bytes 1572864 | tf_op jit(solution)/shard_map/all_to_all | solution.py:132
  24.4 31.5 %collective-permute-start = (bf16[8,64]{1,0:T(8,128)(2,1)S(1)}, bf16[8,64]{1,0:T(8,128)(2,1)S(1)}, u32[]{:S(2)}, u32[]{:S(2)}) collective-permute-start(bf16[8,64]{1,0:T(8,128)(2,1)S(1)} %bitcast.102), channel_id=1, source_target_pairs={{0,64},{64,128},{128,192},{192,256},{256,320},{320,384},{384,448},... | collective-permute-start | bytes 3080 | tf_op jit(solution)/shard_map/ppermute | solution.py:125
  28.3 34.3 %collective-permute-start.1 = (bf16[8,64]{1,0:T(8,128)(2,1)S(1)}, bf16[8,64]{1,0:T(8,128)(2,1)S(1)}, u32[]{:S(2)}, u32[]{:S(2)}) collective-permute-start(bf16[8,64]{1,0:T(8,128)(2,1)S(1)} %bitcast.101), channel_id=1, source_target_pairs={{0,128},{64,192},{128,256},{192,320},{256,384},{320,448},{384,0},{... | collective-permute-start | bytes 3080 | tf_op jit(solution)/shard_map/ppermute | solution.py:125
  35.3 33.3 %collective-permute-start.2 = (bf16[8,64]{1,0:T(8,128)(2,1)S(1)}, bf16[8,64]{1,0:T(8,128)(2,1)S(1)}, u32[]{:S(2)}, u32[]{:S(2)}) collective-permute-start(bf16[8,64]{1,0:T(8,128)(2,1)S(1)} %bitcast.100), channel_id=1, source_target_pairs={{0,192},{64,256},{128,320},{192,384},{256,448},{320,0},{384,64},{4... | collective-permute-start | bytes 3080 | tf_op jit(solution)/shard_map/ppermute | solution.py:125
  40.7 34.3 %collective-permute-start.3 = (bf16[8,64]{1,0:T(8,128)(2,1)S(1)}, bf16[8,64]{1,0:T(8,128)(2,1)S(1)}, u32[]{:S(2)}, u32[]{:S(2)}) collective-permute-start(bf16[8,64]{1,0:T(8,128)(2,1)S(1)} %bitcast.98), channel_id=1, source_target_pairs={{0,256},{64,320},{128,384},{192,448},{256,0},{320,64},{384,128},{4... | collective-permute-start | bytes 3080 | tf_op jit(solution)/shard_map/ppermute | solution.py:125
  47.5 27.5 %collective-permute-start.4 = (bf16[8,64]{1,0:T(8,128)(2,1)S(1)}, bf16[8,64]{1,0:T(8,128)(2,1)S(1)}, u32[]{:S(2)}, u32[]{:S(2)}) collective-permute-start(bf16[8,64]{1,0:T(8,128)(2,1)S(1)} %bitcast.99), channel_id=1, source_target_pairs={{0,320},{64,384},{128,448},{192,0},{256,64},{320,128},{384,192},{4... | collective-permute-start | bytes 3080 | tf_op jit(solution)/shard_map/ppermute | solution.py:125
  56.0 19.1 %collective-permute-start.5 = (bf16[8,64]{1,0:T(8,128)(2,1)S(1)}, bf16[8,64]{1,0:T(8,128)(2,1)S(1)}, u32[]{:S(2)}, u32[]{:S(2)}) collective-permute-start(bf16[8,64]{1,0:T(8,128)(2,1)S(1)} %bitcast.103), channel_id=1, source_target_pairs={{0,384},{64,448},{128,0},{192,64},{256,128},{320,192},{384,256},{4... | collective-permute-start | bytes 3080 | tf_op jit(solution)/shard_map/ppermute | solution.py:125
  64.2 50.0 %copy-start = (bf16[64,48,128]{2,1,0:T(8,128)(2,1)}, bf16[64,48,128]{2,1,0:T(8,128)(2,1)S(1)}, u32[]{:S(2)}) copy-start(bf16[64,48,128]{2,1,0:T(8,128)(2,1)S(1)} %all-to-all-done.refs_0_) | copy-start | bytes 2359300
  64.2 18.8 %collective-permute-start.8 = (bf16[64,48,128]{2,1,0:T(8,128)(2,1)S(1)}, bf16[64,48,128]{2,1,0:T(8,128)(2,1)}, u32[]{:S(2)}, u32[]{:S(2)}) collective-permute-start(bf16[64,48,128]{2,1,0:T(8,128)(2,1)S(1)} %all-to-all-done.refs_0_), channel_id=1, source_target_pairs={{0,2},{1,7},{2,4},{3,1},{4,6},{5,3},{6,0},{7,5},{8,10},{9,15},{10,... | collective-permute-start | bytes 2359304 | tf_op jit(solution)/shard_map/ppermute | solution.py:106
  68.6 17.8 %collective-permute-start.7 = (bf16[64,48,128]{2,1,0:T(8,128)(2,1)S(1)}, bf16[64,48,128]{2,1,0:T(8,128)(2,1)}, u32[]{:S(2)}, u32[]{:S(2)}) collective-permute-start(bf16[64,48,128]{2,1,0:T(8,128)(2,1)S(1)} %all-to-all-done.refs_0_), channel_id=1, source_target_pairs={{0,1},{1,0},{2,3},{3,2},{4,5},{5,4},{6,7},{7,6},{8,9},{9,8},{10,11... | collective-permute-start | bytes 2359304 | tf_op jit(solution)/shard_map/ppermute | solution.py:109
  75.1 38.9 %all-to-all-start.1 = ((bf16[64,32,128]{2,1,0:T(8,128)(2,1)}), bf16[64,32,128]{2,1,0:T(8,128)(2,1)S(1)}, u32[]{:S(2)}, u32[]{:S(2)}) async-start(bf16[64,32,128]{2,1,0:T(8,128)(2,1)} %reshape.480), calls=%async_computation.1 | async-start | bytes 1048576 | tf_op jit(solution)/shard_map/all_to_all | solution.py:186
  83.0 13.3 %collective-permute-start.12 = (bf16[64,48,128]{2,1,0:T(8,128)(2,1)}, bf16[64,48,128]{2,1,0:T(8,128)(2,1)}, u32[]{:S(2)}, u32[]{:S(2)}) collective-permute-start(bf16[64,48,128]{2,1,0:T(8,128)(2,1)} %collective-permute-done.8.refs_2_), channel_id=1, source_target_pairs={{0,2},{1,7},{2,4},{3,1},{4,6},{5,3},{6,0},{7,5},{8,10},{9,15},{10,... | collective-permute-start | bytes 2359304 | tf_op jit(solution)/shard_map/ppermute | solution.py:106
  86.4 18.4 %collective-permute-start.10 = (bf16[64,48,128]{2,1,0:T(8,128)(2,1)}, bf16[64,48,128]{2,1,0:T(8,128)(2,1)}, u32[]{:S(2)}, u32[]{:S(2)}) collective-permute-start(bf16[64,48,128]{2,1,0:T(8,128)(2,1)} %collective-permute-done.7.refs_1_), channel_id=1, source_target_pairs={{0,2},{1,7},{2,4},{3,1},{4,6},{5,3},{6,0},{7,5},{8,10},{9,15},{10,... | collective-permute-start | bytes 2359304 | tf_op jit(solution)/shard_map/ppermute | solution.py:106
  89.6 24.7 %collective-permute-start.9 = (bf16[64,48,128]{2,1,0:T(8,128)(2,1)}, bf16[64,48,128]{2,1,0:T(8,128)(2,1)}, u32[]{:S(2)}, u32[]{:S(2)}) collective-permute-start(bf16[64,48,128]{2,1,0:T(8,128)(2,1)} %collective-permute-done.8.refs_2_), channel_id=1, source_target_pairs={{0,1},{1,0},{2,3},{3,2},{4,5},{5,4},{6,7},{7,6},{8,9},{9,8},{10,11... | collective-permute-start | bytes 2359304 | tf_op jit(solution)/shard_map/ppermute | solution.py:109
  96.3 17.9 %collective-permute-start.13 = (bf16[64,48,128]{2,1,0:T(8,128)(2,1)}, bf16[64,48,128]{2,1,0:T(8,128)(2,1)S(1)}, u32[]{:S(2)}, u32[]{:S(2)}) collective-permute-start(bf16[64,48,128]{2,1,0:T(8,128)(2,1)} %collective-permute-done.12.refs_6_), channel_id=1, source_target_pairs={{0,1},{1,0},{2,3},{3,2},{4,5},{5,4},{6,7},{7,6},{8,9},{9,8},{10,11... | collective-permute-start | bytes 2359304 | tf_op jit(solution)/shard_map/ppermute | solution.py:109
  104.8 9.5 %collective-permute-start.11 = (bf16[64,48,128]{2,1,0:T(8,128)(2,1)}, bf16[64,48,128]{2,1,0:T(8,128)(2,1)S(1)}, u32[]{:S(2)}, u32[]{:S(2)}) collective-permute-start(bf16[64,48,128]{2,1,0:T(8,128)(2,1)} %collective-permute-done.10.refs_4_), channel_id=1, source_target_pairs={{0,1},{1,0},{2,3},{3,2},{4,5},{5,4},{6,7},{7,6},{8,9},{9,8},{10,11... | collective-permute-start | bytes 2359304 | tf_op jit(solution)/shard_map/ppermute | solution.py:109
  118.7 22.4 %all-to-all-start.2 = ((bf16[64,16,256]{2,1,0:T(8,128)(2,1)}), bf16[64,16,256]{2,1,0:T(8,128)(2,1)S(1)}, u32[]{:S(2)}, u32[]{:S(2)}) async-start(bf16[64,16,256]{2,1,0:T(8,128)(2,1)} %expert.1), calls=%async_computation.2 | async-start | bytes 1048576 | tf_op jit(solution)/shard_map/all_to_all | solution.py:201
  128.9 5.5 %collective-permute-start.6 = (bf16[8,64]{1,0:T(8,128)(2,1)S(1)}, bf16[8,64]{1,0:T(8,128)(2,1)S(1)}, u32[]{:S(2)}, u32[]{:S(2)}) collective-permute-start(bf16[8,64]{1,0:T(8,128)(2,1)S(1)} %bitcast.104), channel_id=1, source_target_pairs={{0,448},{64,0},{128,64},{192,128},{256,192},{320,256},{384,320},{4... | collective-permute-start | bytes 3080 | tf_op jit(solution)/shard_map/ppermute | solution.py:125
  141.1 6.9 %copy-start.1 = (bf16[64,48,128]{2,1,0:T(8,128)(2,1)S(1)}, bf16[64,48,128]{2,1,0:T(8,128)(2,1)}, u32[]{:S(2)}) copy-start(bf16[64,48,128]{2,1,0:T(8,128)(2,1)} %copy-done) | copy-start | bytes 2359300
  142.5 25.2 %all-to-all-start.3 = ((bf16[8,64,256]{2,1,0:T(8,128)(2,1)}), bf16[8,64,256]{2,1,0:T(8,128)(2,1)S(1)}, u32[]{:S(2)}, u32[]{:S(2)}) async-start(bf16[8,64,256]{2,1,0:T(8,128)(2,1)} %bitcast.36), calls=%async_computation.3 | async-start | bytes 524288 | tf_op jit(solution)/shard_map/all_to_all | solution.py:205

commit v5 on v4

--- a/solution.py
+++ b/solution.py
@@ -14,7 +14,7 @@
 F32 = jnp.float32
 
 
-HELD = (0, 6, 8)
+HELD = (0, 2, 6, 8)
 
 
 def pack_kernel(gain_ref, gate_ref, up_ref, down_ref, out_ref):
@@ -97,22 +97,20 @@
 
 
 def gather_weights(own):
-    around = []
-    for i in range(4):
-        around.append((2 * i, 2 * ((i + 1) % 4)))
-        around.append((2 * i + 1, 2 * ((i + 3) % 4) + 1))
-
-    def pass_on(v):
-        return lax.ppermute(v, TP, around)
+    ring = [(i, (i + 1) % 4) for i in range(4)]
+    around = [pair for i, j in ring for pair in ((2 * i, 2 * j), (2 * j + 1, 2 * i + 1))]
+    back = [(j, i) for i, j in around]
+
+    def pass_on(v, pairs):
+        return lax.ppermute(v, TP, pairs)
 
     def swap(v):
         return lax.ppermute(v, "c", [(0, 1), (1, 0)])
 
-    near = pass_on(own)
-    own_c = swap(own)
-    other = pass_on(own_c)
-    far = pass_on(near)
-    near_c, other_c, far_c = swap(near), swap(other), swap(far)
+    near, other = pass_on(own, around), pass_on(own, back)
+    far = pass_on(near, around)
+    own_c, near_c = swap(own), swap(near)
+    other_c, far_c = swap(other), swap(far)
     return own, own_c, near, near_c, other, other_c, far, far_c
 
 

time: 170 us -> 172 us (1.012)
  starting transfers between devices: 108 us -> 119 us
  waiting for transfers between devices: 40.5 us -> 30.6 us
  local copies, waits for them, and re-layouts: 4.91 us -> 7.18 us
    ppermute x3, waiting for transfers between devices: 7.68 us -> 1.25 us  [pass_on(): return lax.ppermute(v, TP, pairs)]
    all_to_all x1, waiting for transfers between devices: 4.51 us -> 0.01 us  [local(): lax.all_to_all(sent, ('l', 'y', 'g'), split_axis=0, concat_axis=0, tiled=...]
    ppermute x4, starting transfers between devices: 17.5 us -> 21.3 us  [swap(): return lax.ppermute(v, 'c', [(0, 1), (1, 0)])]
    all_to_all x1, starting transfers between devices: 4.97 us -> 8.42 us  [local(): lax.all_to_all(mixed.reshape(8, 64, 256), 'g', split_axis=0, concat_axis=...]
    all_to_all x1, starting transfers between devices: 7.9 us -> 10.6 us  [local(): lax.all_to_all(sent, ('l', 'y', 'g'), split_axis=0, concat_axis=0, tiled=...]
    all_to_all x1, waiting for transfers between devices: 16.4 us -> 14.1 us  [local(): lax.all_to_all(mixed.reshape(8, 64, 256), 'g', split_axis=0, concat_axis=...]
    ppermute x4, waiting for transfers between devices: 0.01 us -> 2.2 us  [swap(): return lax.ppermute(v, 'c', [(0, 1), (1, 0)])]
  transfers between devices with their start and end apart: 18 -> 18, of which waited for: 8 -> 7; matrix products, arithmetic and copies ran while one was open for 5% -> 6% of each run, Pallas kernels for 0% -> 0%
where the time goes in v5:
time: 172 us; the launch traced here: 171 us
  starting transfers between devices  119 us (69%)
  waiting for transfers between devices  30.6 us (18%)
  Pallas kernels  9.49 us (6%)
  local copies, waits for them, and re-layouts  7.18 us (4%)
  matrix products  2.69 us (2%)
    ppermute x7, starting transfers between devices, trade_facts(): part = lax.ppermute(part, 'g', [(i, (i + k) % 8) for i in range(8)])  37.5 us
    ppermute x4, starting transfers between devices, swap(): return lax.ppermute(v, 'c', [(0, 1), (1, 0)])  21.3 us
    all_to_all x1, starting transfers between devices, local(): own = lax.all_to_all(packed, FS, split_axis=0, concat_axis=0, tiled=True)  19.6 us
    all_to_all x1, waiting for transfers between devices, local(): lax.all_to_all(mixed.reshape(8, 64, 256), 'g', split_axis=0, concat_axis=...  14.1 us
    ppermute x3, starting transfers between devices, pass_on(): return lax.ppermute(v, TP, pairs)  10.9 us
    all_to_all x1, starting transfers between devices, local(): lax.all_to_all(sent, ('l', 'y', 'g'), split_axis=0, concat_axis=0, tiled=...  10.6 us
    all_to_all x1, starting transfers between devices, local(): lax.all_to_all(outs, IN_GROUP, split_axis=0, concat_axis=0, tiled=True)  10.1 us
    all_to_all x1, starting transfers between devices, local(): lax.all_to_all(mixed.reshape(8, 64, 256), 'g', split_axis=0, concat_axis=...  8.42 us
  transfers between devices with their start and end apart: 18, of which 7 were waited for; matrix products, arithmetic and copies ran while one was open for 6% of the time, Pallas kernels for 0%

profile of v5, /device:TPU:1, one launch (start us, length us, event | category | flops | bytes accessed | tf_op | source)
XLA Modules:
  0.0 170.7 jit_solution(3689966653998246611)
XLA Ops:
  0.6 0.0 copy-start.1
  0.6 3.4 %pack.1 = bf16[64,48,128]{2,1,0:T(8,128)(2,1)} custom-call(f32[1,32]{1,0:T(1,128)} %bitcast.109, f32[64,32,64]{2,1,0:T(8,128)} %gate_ref.1, f32[64,32,64]{2,1,0:T(8,128)} %up_ref.1, f32[64,32,64]{2,1,0:T(8,128)} %down_ref.1), custom_call_target="tpu_custom_call" | custom-call | tf_op jit(solution)/shard_map/pack/pallas_call | solution.py:33
  4.0 19.6 %all-to-all-start = ((bf16[64,48,128]{2,1,0:T(8,128)(2,1)}), bf16[64,48,128]{2,1,0:T(8,128)(2,1)}, u32[]{:S(2)}, u32[]{:S(2)}) async-start(bf16[64,48,128]{2,1,0:T(8,128)(2,1)} %pack.1), calls=%async_computation | async-start | bytes 1572864 | tf_op jit(solution)/shard_map/all_to_all | solution.py:130
  23.7 0.0 copy-done.1
  23.7 0.3 select_reduce_fusion.1
  24.1 0.0 copy-done.2
  24.1 0.0 copy-done.3
  24.3 0.3 convolution_convert_fusion.1
  24.6 0.1 reshape.479
  24.7 3.8 %collective-permute-start = (bf16[8,64]{1,0:T(8,128)(2,1)S(1)}, bf16[8,64]{1,0:T(8,128)(2,1)S(1)}, u32[]{:S(2)}, u32[]{:S(2)}) collective-permute-start(bf16[8,64]{1,0:T(8,128)(2,1)S(1)} %bitcast.102), channel_id=1, source_target_pairs={{0,64},{64,128},{128,192},{192,256},{256,320},{320,384},{384,448},... | collective-permute-start | bytes 3080 | tf_op jit(solution)/shard_map/ppermute | solution.py:123
  28.5 7.0 %collective-permute-start.1 = (bf16[8,64]{1,0:T(8,128)(2,1)S(1)}, bf16[8,64]{1,0:T(8,128)(2,1)S(1)}, u32[]{:S(2)}, u32[]{:S(2)}) collective-permute-start(bf16[8,64]{1,0:T(8,128)(2,1)S(1)} %bitcast.101), channel_id=1, source_target_pairs={{0,128},{64,192},{128,256},{192,320},{256,384},{320,448},{384,0},{... | collective-permute-start | bytes 3080 | tf_op jit(solution)/shard_map/ppermute | solution.py:123
  35.6 5.4 %collective-permute-start.2 = (bf16[8,64]{1,0:T(8,128)(2,1)S(1)}, bf16[8,64]{1,0:T(8,128)(2,1)S(1)}, u32[]{:S(2)}, u32[]{:S(2)}) collective-permute-start(bf16[8,64]{1,0:T(8,128)(2,1)S(1)} %bitcast.98), channel_id=1, source_target_pairs={{0,192},{64,256},{128,320},{192,384},{256,448},{320,0},{384,64},{4... | collective-permute-start | bytes 3080 | tf_op jit(solution)/shard_map/ppermute | solution.py:123
  41.0 6.8 %collective-permute-start.3 = (bf16[8,64]{1,0:T(8,128)(2,1)S(1)}, bf16[8,64]{1,0:T(8,128)(2,1)S(1)}, u32[]{:S(2)}, u32[]{:S(2)}) collective-permute-start(bf16[8,64]{1,0:T(8,128)(2,1)S(1)} %bitcast.99), channel_id=1, source_target_pairs={{0,256},{64,320},{128,384},{192,448},{256,0},{320,64},{384,128},{4... | collective-permute-start | bytes 3080 | tf_op jit(solution)/shard_map/ppermute | solution.py:123
  47.8 5.5 %collective-permute-start.4 = (bf16[8,64]{1,0:T(8,128)(2,1)S(1)}, bf16[8,64]{1,0:T(8,128)(2,1)S(1)}, u32[]{:S(2)}, u32[]{:S(2)}) collective-permute-start(bf16[8,64]{1,0:T(8,128)(2,1)S(1)} %bitcast.100), channel_id=1, source_target_pairs={{0,320},{64,384},{128,448},{192,0},{256,64},{320,128},{384,192},{4... | collective-permute-start | bytes 3080 | tf_op jit(solution)/shard_map/ppermute | solution.py:123
  53.3 0.0 copy-done
  53.3 0.5 multiply_reduce_fusion
  53.8 2.3 %collective-permute-done = bf16[8,64]{1,0:T(8,128)(2,1)S(1)} collective-permute-done((bf16[8,64]{1,0:T(8,128)(2,1)S(1)}, bf16[8,64]{1,0:T(8,128)(2,1)S(1)}, u32[]{:S(2)}, u32[]{:S(2)}) %collective-permute-start) | collective-permute-done | bytes 1056 | tf_op jit(solution)/shard_map/ppermute | solution.py:123
  56.1 6.6 %collective-permute-start.5 = (bf16[8,64]{1,0:T(8,128)(2,1)S(1)}, bf16[8,64]{1,0:T(8,128)(2,1)S(1)}, u32[]{:S(2)}, u32[]{:S(2)}) collective-permute-start(bf16[8,64]{1,0:T(8,128)(2,1)S(1)} %bitcast.103), channel_id=1, source_target_pairs={{0,384},{64,448},{128,0},{192,64},{256,128},{320,192},{384,256},{4... | collective-permute-start | bytes 3080 | tf_op jit(solution)/shard_map/ppermute | solution.py:123
  62.8 0.0 collective-permute-done.1
  62.8 1.6 all-to-all-done.refs_0_
  64.4 4.4 %collective-permute-start.8 = (bf16[64,48,128]{2,1,0:T(8,128)(2,1)}, bf16[64,48,128]{2,1,0:T(8,128)(2,1)}, u32[]{:S(2)}, u32[]{:S(2)}) collective-permute-start(bf16[64,48,128]{2,1,0:T(8,128)(2,1)} %all-to-all-done.refs_0_), channel_id=1, source_target_pairs={{0,2},{3,1},{2,4},{5,3},{4,6},{7,5},{6,0},{1,7},{8,10},{11,9},{10,... | collective-permute-start | bytes 2359304 | tf_op jit(solution)/shard_map/ppermute | solution.py:105
  68.8 0.1 multiply_convert_fusion
  68.9 1.0 reshape.480
  70.0 0.0 collective-permute-done.2
  70.0 0.0 collective-permute-done.3
  70.0 0.0 collective-permute-done.4
  70.0 0.0 collective-permute-done.5
  70.0 10.6 %all-to-all-start.1 = ((bf16[64,32,128]{2,1,0:T(8,128)(2,1)}), bf16[64,32,128]{2,1,0:T(8,128)(2,1)S(1)}, u32[]{:S(2)}, u32[]{:S(2)}) async-start(bf16[64,32,128]{2,1,0:T(8,128)(2,1)} %reshape.480), calls=%async_computation.1 | async-start | bytes 1048576 | tf_op jit(solution)/shard_map/all_to_all | solution.py:184
  80.6 3.1 %collective-permute-start.10 = (bf16[64,48,128]{2,1,0:T(8,128)(2,1)}, bf16[64,48,128]{2,1,0:T(8,128)(2,1)}, u32[]{:S(2)}, u32[]{:S(2)}) collective-permute-start(bf16[64,48,128]{2,1,0:T(8,128)(2,1)} %all-to-all-done.refs_0_), channel_id=1, source_target_pairs={{2,0},{1,3},{4,2},{3,5},{6,4},{5,7},{0,6},{7,1},{10,8},{9,11},{12,... | collective-permute-start | bytes 2359304 | tf_op jit(solution)/shard_map/ppermute | solution.py:105
  83.8 0.0 collective-permute-done.8.refs_2_
  83.8 3.4 %collective-permute-start.12 = (bf16[64,48,128]{2,1,0:T(8,128)(2,1)}, bf16[64,48,128]{2,1,0:T(8,128)(2,1)}, u32[]{:S(2)}, u32[]{:S(2)}) collective-permute-start(bf16[64,48,128]{2,1,0:T(8,128)(2,1)} %collective-permute-done.8.refs_2_), channel_id=1, source_target_pairs={{0,2},{3,1},{2,4},{5,3},{4,6},{7,5},{6,0},{1,7},{8,10},{11,9},{10,... | collective-permute-start | bytes 2359304 | tf_op jit(solution)/shard_map/ppermute | solution.py:105
  87.1 5.1 %collective-permute-start.7 = (bf16[64,48,128]{2,1,0:T(8,128)(2,1)}, bf16[64,48,128]{2,1,0:T(8,128)(2,1)S(1)}, u32[]{:S(2)}, u32[]{:S(2)}) collective-permute-start(bf16[64,48,128]{2,1,0:T(8,128)(2,1)} %all-to-all-done.refs_0_), channel_id=1, source_target_pairs={{0,1},{1,0},{2,3},{3,2},{4,5},{5,4},{6,7},{7,6},{8,9},{9,8},{10,11... | collective-permute-start | bytes 2359304 | tf_op jit(solution)/shard_map/ppermute | solution.py:108
  92.2 1.9 %collective-permute-start.9 = (bf16[64,48,128]{2,1,0:T(8,128)(2,1)}, bf16[64,48,128]{2,1,0:T(8,128)(2,1)}, u32[]{:S(2)}, u32[]{:S(2)}) collective-permute-start(bf16[64,48,128]{2,1,0:T(8,128)(2,1)} %collective-permute-done.8.refs_2_), channel_id=1, source_target_pairs={{0,1},{1,0},{2,3},{3,2},{4,5},{5,4},{6,7},{7,6},{8,9},{9,8},{10,11... | collective-permute-start | bytes 2359304 | tf_op jit(solution)/shard_map/ppermute | solution.py:108
  94.1 1.2 collective-permute-done.10.refs_4_
  95.4 12.4 %collective-permute-start.11 = (bf16[64,48,128]{2,1,0:T(8,128)(2,1)}, bf16[64,48,128]{2,1,0:T(8,128)(2,1)S(1)}, u32[]{:S(2)}, u32[]{:S(2)}) collective-permute-start(bf16[64,48,128]{2,1,0:T(8,128)(2,1)} %collective-permute-done.10.refs_4_), channel_id=1, source_target_pairs={{0,1},{1,0},{2,3},{3,2},{4,5},{5,4},{6,7},{7,6},{8,9},{9,8},{10,11... | collective-permute-start | bytes 2359304 | tf_op jit(solution)/shard_map/ppermute | solution.py:108
  107.8 0.0 collective-permute-done.12.refs_6_
  107.8 1.9 %collective-permute-start.13 = (bf16[64,48,128]{2,1,0:T(8,128)(2,1)}, bf16[64,48,128]{2,1,0:T(8,128)(2,1)S(1)}, u32[]{:S(2)}, u32[]{:S(2)}) collective-permute-start(bf16[64,48,128]{2,1,0:T(8,128)(2,1)} %collective-permute-done.12.refs_6_), channel_id=1, source_target_pairs={{0,1},{1,0},{2,3},{3,2},{4,5},{5,4},{6,7},{7,6},{8,9},{9,8},{10,11... | collective-permute-start | bytes 2359304 | tf_op jit(solution)/shard_map/ppermute | solution.py:108
  109.8 0.0 all-to-all-done.1
  109.8 0.2 reshape.481.x_ref
  110.0 0.0 collective-permute-done.7.refs_1_
  110.0 0.0 collective-permute-done.9.refs_3_
  110.0 0.0 collective-permute-done.11.refs_5_
  110.0 2.2 %collective-permute-done.13.refs_7_ = bf16[64,48,128]{2,1,0:T(8,128)(2,1)S(1)} collective-permute-done((bf16[64,48,128]{2,1,0:T(8,128)(2,1)}, bf16[64,48,128]{2,1,0:T(8,128)(2,1)S(1)}, u32[]{:S(2)}, u32[]{:S(2)}) %collective-permute-start.13) | collective-permute-done | bytes 786464 | tf_op jit(solution)/shard_map/ppermute | solution.py:108
  112.2 4.2 %expert.1 = bf16[64,16,256]{2,1,0:T(8,128)(2,1)} custom-call(bf16[128,2048]{1,0:T(8,128)(2,1)S(1)} %reshape.481.x_ref, bf16[64,48,128]{2,1,0:T(8,128)(2,1)} %all-to-all-done.refs_0_, bf16[64,48,128]{2,1,0:T(8,128)(2,1)S(1)} %collective-permute-done.7.refs_1_, bf16[64,48,128]{2,1,0:T(8,128)(2,1)} %collective-permute-done.8.refs_2_, ...), custom_call_target="tpu_custom_call" | custom-call | tf_op jit(solution)/shard_map/expert/pallas_call | solution.py:91
  116.5 10.1 %all-to-all-start.2 = ((bf16[64,16,256]{2,1,0:T(8,128)(2,1)}), bf16[64,16,256]{2,1,0:T(8,128)(2,1)S(1)}, u32[]{:S(2)}, u32[]{:S(2)}) async-start(bf16[64,16,256]{2,1,0:T(8,128)(2,1)} %expert.1), calls=%async_computation.2 | async-start | bytes 1048576 | tf_op jit(solution)/shard_map/all_to_all | solution.py:199
  126.6 2.5 %collective-permute-start.6 = (bf16[8,64]{1,0:T(8,128)(2,1)S(1)}, bf16[8,64]{1,0:T(8,128)(2,1)S(1)}, u32[]{:S(2)}, u32[]{:S(2)}) collective-permute-start(bf16[8,64]{1,0:T(8,128)(2,1)S(1)} %bitcast.104), channel_id=1, source_target_pairs={{0,448},{64,0},{128,64},{192,128},{256,192},{320,256},{384,320},{4... | collective-permute-start | bytes 3080 | tf_op jit(solution)/shard_map/ppermute | solution.py:123
  129.2 2.9 %collective-permute-done.6 = bf16[8,64]{1,0:T(8,128)(2,1)S(1)} collective-permute-done((bf16[8,64]{1,0:T(8,128)(2,1)S(1)}, bf16[8,64]{1,0:T(8,128)(2,1)S(1)}, u32[]{:S(2)}, u32[]{:S(2)}) %collective-permute-start.6) | collective-permute-done | bytes 1056 | tf_op jit(solution)/shard_map/ppermute | solution.py:123
  132.1 0.1 stack.53
  132.2 0.2 convolution_bitcast_fusion
  132.4 0.1 convert_element_type.111
  132.5 0.1 broadcast_in_dim.50
  132.6 0.1 broadcast_in_dim.52
  132.7 6.1 %all-to-all-done.2 = bf16[64,16,256]{2,1,0:T(8,128)(2,1)S(1)} async-done(((bf16[64,16,256]{2,1,0:T(8,128)(2,1)}), bf16[64,16,256]{2,1,0:T(8,128)(2,1)S(1)}, u32[]{:S(2)}, u32[]{:S(2)}) %all-to-all-start.2) | async-done | bytes 524320 | tf_op jit(solution)/shard_map/all_to_all | solution.py:199
  138.8 1.3 convolution_convert_fusion
  140.2 8.4 %all-to-all-start.3 = ((bf16[8,64,256]{2,1,0:T(8,128)(2,1)}), bf16[8,64,256]{2,1,0:T(8,128)(2,1)S(1)}, u32[]{:S(2)}, u32[]{:S(2)}) async-start(bf16[8,64,256]{2,1,0:T(8,128)(2,1)} %bitcast.36), calls=%async_computation.3 | async-start | bytes 524288 | tf_op jit(solution)/shard_map/all_to_all | solution.py:203
  148.6 0.6 multiply_add_fusion.1.slot_ref
  149.2 1.2 fusion.50
  150.4 0.1 pad_maximum_fusion
  150.5 0.9 copy.31
  151.4 1.4 fusion.51
  152.8 0.9 copy.29
  153.7 0.9 copy.30
  154.6 14.1 %all-to-all-done.3 = bf16[8,64,256]{2,1,0:T(8,128)(2,1)S(1)} async-done(((bf16[8,64,256]{2,1,0:T(8,128)(2,1)}), bf16[8,64,256]{2,1,0:T(8,128)(2,1)S(1)}, u32[]{:S(2)}, u32[]{:S(2)}) %all-to-all-start.3) | async-done | bytes 262176 | tf_op jit(solution)/shard_map/all_to_all | solution.py:203
  168.8 1.9 %home.1 = bf16[512,256]{1,0:T(8,128)(2,1)} custom-call(s32[1,512]{1,0:T(1,128)} %multiply_add_fusion.1.slot_ref, bf16[512,256]{1,0:T(8,128)(2,1)S(1)} %bitcast.76), custom_call_target="tpu_custom_call" | custom-call | tf_op jit(solution)/shard_map/home/pallas_call | solution.py:206
  (40 shorter events, 0.4 us)
Async XLA Ops:
  0.6 23.1 %copy-start.1 = (s32[512,2]{0,1:T(2,128)S(1)}, s32[512,2]{0,1:T(2,128)}, u32[]{:S(2)}) copy-start(s32[512,2]{0,1:T(2,128)} %param.13) | copy-start | bytes 12292
  4.0 20.0 %copy-start.2 = (f32[512,2]{0,1:T(2,128)S(1)}, f32[512,2]{0,1:T(2,128)}, u32[]{:S(2)}) copy-start(f32[512,2]{0,1:T(2,128)} %param.15) | copy-start | bytes 12292
  4.0 20.1 %copy-start.3 = (f32[512]{0:T(512)S(1)}, f32[512]{0:T(512)}, u32[]{:S(2)}) copy-start(f32[512]{0:T(512)} %param.14) | copy-start | bytes 6148
  4.0 49.3 %copy-start = (bf16[512,2048]{1,0:T(8,128)(2,1)S(1)}, bf16[512,2048]{1,0:T(8,128)(2,1)}, u32[]{:S(2)}) copy-start(bf16[512,2048]{1,0:T(8,128)(2,1)} %param.8) | copy-start | bytes 6291460
  4.0 60.4 %all-to-all-start = ((bf16[64,48,128]{2,1,0:T(8,128)(2,1)}), bf16[64,48,128]{2,1,0:T(8,128)(2,1)}, u32[]{:S(2)}, u32[]{:S(2)}) async-start(bf16[64,48,128]{2,1,0:T(8,128)(2,1)} %pack.1), calls=%async_computation | async-start | bytes 1572864 | tf_op jit(solution)/shard_map/all_to_all | solution.py:130
  24.7 31.4 %collective-permute-start = (bf16[8,64]{1,0:T(8,128)(2,1)S(1)}, bf16[8,64]{1,0:T(8,128)(2,1)S(1)}, u32[]{:S(2)}, u32[]{:S(2)}) collective-permute-start(bf16[8,64]{1,0:T(8,128)(2,1)S(1)} %bitcast.102), channel_id=1, source_target_pairs={{0,64},{64,128},{128,192},{192,256},{256,320},{320,384},{384,448},... | collective-permute-start | bytes 3080 | tf_op jit(solution)/shard_map/ppermute | solution.py:123
  28.5 34.3 %collective-permute-start.1 = (bf16[8,64]{1,0:T(8,128)(2,1)S(1)}, bf16[8,64]{1,0:T(8,128)(2,1)S(1)}, u32[]{:S(2)}, u32[]{:S(2)}) collective-permute-start(bf16[8,64]{1,0:T(8,128)(2,1)S(1)} %bitcast.101), channel_id=1, source_target_pairs={{0,128},{64,192},{128,256},{192,320},{256,384},{320,448},{384,0},{... | collective-permute-start | bytes 3080 | tf_op jit(solution)/shard_map/ppermute | solution.py:123
  35.6 34.4 %collective-permute-start.2 = (bf16[8,64]{1,0:T(8,128)(2,1)S(1)}, bf16[8,64]{1,0:T(8,128)(2,1)S(1)}, u32[]{:S(2)}, u32[]{:S(2)}) collective-permute-start(bf16[8,64]{1,0:T(8,128)(2,1)S(1)} %bitcast.98), channel_id=1, source_target_pairs={{0,192},{64,256},{128,320},{192,384},{256,448},{320,0},{384,64},{4... | collective-permute-start | bytes 3080 | tf_op jit(solution)/shard_map/ppermute | solution.py:123
  41.0 29.0 %collective-permute-start.3 = (bf16[8,64]{1,0:T(8,128)(2,1)S(1)}, bf16[8,64]{1,0:T(8,128)(2,1)S(1)}, u32[]{:S(2)}, u32[]{:S(2)}) collective-permute-start(bf16[8,64]{1,0:T(8,128)(2,1)S(1)} %bitcast.99), channel_id=1, source_target_pairs={{0,256},{64,320},{128,384},{192,448},{256,0},{320,64},{384,128},{4... | collective-permute-start | bytes 3080 | tf_op jit(solution)/shard_map/ppermute | solution.py:123
  47.8 22.2 %collective-permute-start.4 = (bf16[8,64]{1,0:T(8,128)(2,1)S(1)}, bf16[8,64]{1,0:T(8,128)(2,1)S(1)}, u32[]{:S(2)}, u32[]{:S(2)}) collective-permute-start(bf16[8,64]{1,0:T(8,128)(2,1)S(1)} %bitcast.100), channel_id=1, source_target_pairs={{0,320},{64,384},{128,448},{192,0},{256,64},{320,128},{384,192},{4... | collective-permute-start | bytes 3080 | tf_op jit(solution)/shard_map/ppermute | solution.py:123
  56.1 13.8 %collective-permute-start.5 = (bf16[8,64]{1,0:T(8,128)(2,1)S(1)}, bf16[8,64]{1,0:T(8,128)(2,1)S(1)}, u32[]{:S(2)}, u32[]{:S(2)}) collective-permute-start(bf16[8,64]{1,0:T(8,128)(2,1)S(1)} %bitcast.103), channel_id=1, source_target_pairs={{0,384},{64,448},{128,0},{192,64},{256,128},{320,192},{384,256},{4... | collective-permute-start | bytes 3080 | tf_op jit(solution)/shard_map/ppermute | solution.py:123
  64.4 19.4 %collective-permute-start.8 = (bf16[64,48,128]{2,1,0:T(8,128)(2,1)}, bf16[64,48,128]{2,1,0:T(8,128)(2,1)}, u32[]{:S(2)}, u32[]{:S(2)}) collective-permute-start(bf16[64,48,128]{2,1,0:T(8,128)(2,1)} %all-to-all-done.refs_0_), channel_id=1, source_target_pairs={{0,2},{3,1},{2,4},{5,3},{4,6},{7,5},{6,0},{1,7},{8,10},{11,9},{10,... | collective-permute-start | bytes 2359304 | tf_op jit(solution)/shard_map/ppermute | solution.py:105
  70.0 39.8 %all-to-all-start.1 = ((bf16[64,32,128]{2,1,0:T(8,128)(2,1)}), bf16[64,32,128]{2,1,0:T(8,128)(2,1)S(1)}, u32[]{:S(2)}, u32[]{:S(2)}) async-start(bf16[64,32,128]{2,1,0:T(8,128)(2,1)} %reshape.480), calls=%async_computation.1 | async-start | bytes 1048576 | tf_op jit(solution)/shard_map/all_to_all | solution.py:184
  80.6 14.8 %collective-permute-start.10 = (bf16[64,48,128]{2,1,0:T(8,128)(2,1)}, bf16[64,48,128]{2,1,0:T(8,128)(2,1)}, u32[]{:S(2)}, u32[]{:S(2)}) collective-permute-start(bf16[64,48,128]{2,1,0:T(8,128)(2,1)} %all-to-all-done.refs_0_), channel_id=1, source_target_pairs={{2,0},{1,3},{4,2},{3,5},{6,4},{5,7},{0,6},{7,1},{10,8},{9,11},{12,... | collective-permute-start | bytes 2359304 | tf_op jit(solution)/shard_map/ppermute | solution.py:105
  83.8 24.1 %collective-permute-start.12 = (bf16[64,48,128]{2,1,0:T(8,128)(2,1)}, bf16[64,48,128]{2,1,0:T(8,128)(2,1)}, u32[]{:S(2)}, u32[]{:S(2)}) collective-permute-start(bf16[64,48,128]{2,1,0:T(8,128)(2,1)} %collective-permute-done.8.refs_2_), channel_id=1, source_target_pairs={{0,2},{3,1},{2,4},{5,3},{4,6},{7,5},{6,0},{1,7},{8,10},{11,9},{10,... | collective-permute-start | bytes 2359304 | tf_op jit(solution)/shard_map/ppermute | solution.py:105
  87.1 22.9 %collective-permute-start.7 = (bf16[64,48,128]{2,1,0:T(8,128)(2,1)}, bf16[64,48,128]{2,1,0:T(8,128)(2,1)S(1)}, u32[]{:S(2)}, u32[]{:S(2)}) collective-permute-start(bf16[64,48,128]{2,1,0:T(8,128)(2,1)} %all-to-all-done.refs_0_), channel_id=1, source_target_pairs={{0,1},{1,0},{2,3},{3,2},{4,5},{5,4},{6,7},{7,6},{8,9},{9,8},{10,11... | collective-permute-start | bytes 2359304 | tf_op jit(solution)/shard_map/ppermute | solution.py:108
  92.2 17.8 %collective-permute-start.9 = (bf16[64,48,128]{2,1,0:T(8,128)(2,1)}, bf16[64,48,128]{2,1,0:T(8,128)(2,1)}, u32[]{:S(2)}, u32[]{:S(2)}) collective-permute-start(bf16[64,48,128]{2,1,0:T(8,128)(2,1)} %collective-permute-done.8.refs_2_), channel_id=1, source_target_pairs={{0,1},{1,0},{2,3},{3,2},{4,5},{5,4},{6,7},{7,6},{8,9},{9,8},{10,11... | collective-permute-start | bytes 2359304 | tf_op jit(solution)/shard_map/ppermute | solution.py:108
  95.4 14.6 %collective-permute-start.11 = (bf16[64,48,128]{2,1,0:T(8,128)(2,1)}, bf16[64,48,128]{2,1,0:T(8,128)(2,1)S(1)}, u32[]{:S(2)}, u32[]{:S(2)}) collective-permute-start(bf16[64,48,128]{2,1,0:T(8,128)(2,1)} %collective-permute-done.10.refs_4_), channel_id=1, source_target_pairs={{0,1},{1,0},{2,3},{3,2},{4,5},{5,4},{6,7},{7,6},{8,9},{9,8},{10,11... | collective-permute-start | bytes 2359304 | tf_op jit(solution)/shard_map/ppermute | solution.py:108
  107.8 4.4 %collective-permute-start.13 = (bf16[64,48,128]{2,1,0:T(8,128)(2,1)}, bf16[64,48,128]{2,1,0:T(8,128)(2,1)S(1)}, u32[]{:S(2)}, u32[]{:S(2)}) collective-permute-start(bf16[64,48,128]{2,1,0:T(8,128)(2,1)} %collective-permute-done.12.refs_6_), channel_id=1, source_target_pairs={{0,1},{1,0},{2,3},{3,2},{4,5},{5,4},{6,7},{7,6},{8,9},{9,8},{10,11... | collective-permute-start | bytes 2359304 | tf_op jit(solution)/shard_map/ppermute | solution.py:108
  116.5 22.4 %all-to-all-start.2 = ((bf16[64,16,256]{2,1,0:T(8,128)(2,1)}), bf16[64,16,256]{2,1,0:T(8,128)(2,1)S(1)}, u32[]{:S(2)}, u32[]{:S(2)}) async-start(bf16[64,16,256]{2,1,0:T(8,128)(2,1)} %expert.1), calls=%async_computation.2 | async-start | bytes 1048576 | tf_op jit(solution)/shard_map/all_to_all | solution.py:199
  126.6 5.5 %collective-permute-start.6 = (bf16[8,64]{1,0:T(8,128)(2,1)S(1)}, bf16[8,64]{1,0:T(8,128)(2,1)S(1)}, u32[]{:S(2)}, u32[]{:S(2)}) collective-permute-start(bf16[8,64]{1,0:T(8,128)(2,1)S(1)} %bitcast.104), channel_id=1, source_target_pairs={{0,448},{64,0},{128,64},{192,128},{256,192},{320,256},{384,320},{4... | collective-permute-start | bytes 3080 | tf_op jit(solution)/shard_map/ppermute | solution.py:123
  140.2 28.6 %all-to-all-start.3 = ((bf16[8,64,256]{2,1,0:T(8,128)(2,1)}), bf16[8,64,256]{2,1,0:T(8,128)(2,1)S(1)}, u32[]{:S(2)}, u32[]{:S(2)}) async-start(bf16[8,64,256]{2,1,0:T(8,128)(2,1)} %bitcast.36), calls=%async_computation.3 | async-start | bytes 524288 | tf_op jit(solution)/shard_map/all_to_all | solution.py:203
